TPU v7x, 32 devices: a whole 2x2x4 slice. The times are simulated.
32 devices in a mesh: sp: 8 (over z, core), tp: 4 (over y, x).
Axes of the slice: x: 2, y: 2, z: 4, core: 2. Of those that a mesh axis runs over, the one named last changes fastest.
Arguments:
- residual: bfloat16 [1024, 4096], P('sp', 'tp'), may hold values from -46 to 46
- query_small: bfloat16 [1024, 2048], P('sp', 'tp'), may hold values from -6 to 6
- key_narrow_group: bfloat16 [1024, 2048], P('sp', 'tp'), may hold values from -6 to 6
- query_large: bfloat16 [1024, 4096], P('sp', 'tp'), may hold values from -6 to 6
- key_large: bfloat16 [1024, 4096], P('sp', 'tp'), may hold values from -6 to 6
- values: bfloat16 [1024, 2, 2048], P('sp', None, 'tp'), may hold values from -6 to 6
- gates: bfloat16 [1024, 2, 2048], P('sp', None, 'tp'), may hold values from -6 to 6
- log_decay: float32 [1024, 2, 16], P('sp', None, 'tp'), may hold values from -0.65 to 0, as said below
- head_gain: float32 [2, 2048], P(None, 'tp'), may hold values from 0.1 to 1.9
- out_weight: bfloat16 [2, 2048, 4096], P(None, 'sp', 'tp'), may hold values from -0.09375 to 0.09375
- norm_gain: float32 [4096], P('tp'), may hold values from 0.1 to 1.9
- routes: int32 [1024, 2], P('sp'), may hold values from 0 to 7, all different within a row; in each aligned block of 128 rows (0 to 127, 128 to 255, ...) at most 64 rows name the same one
- route_weight: float32 [1024, 2], P('sp'), may hold values from 0.2 to 1
- expert_gate: bfloat16 [8, 4096, 2048], P('sp', None, 'tp'), may hold values from -0.09375 to 0.09375
- expert_up: bfloat16 [8, 4096, 2048], P('sp', None, 'tp'), may hold values from -0.09375 to 0.09375
- expert_down: bfloat16 [8, 2048, 4096], P('sp', None, 'tp'), may hold values from -0.5 to 0.5
Outputs:
- new_stream: bfloat16 [1024, 4096], P('sp', 'tp')
Inputs may be any that keep to these rules, and one draw needn't show every extreme that they name: `routes`: each row names two different experts; in each aligned block of 128 rows no expert is named more than 64 times, a bound that some block reaches. `log_decay`: negative at every position.
All inputs are finite; a program needn't handle non-finite values.
Results may differ from a plain program's by a relative error of at most 0.019.
Values may be sent and summed in bfloat16 or wider, within the bound.
No kernel may reach another device: no remote copies, remote signals or barrier semaphores. Data moves between devices by JAX's collectives and lax.ppermute only.
A program may use at most 64 MiB of HBM per device.

v0:
```python
import functools

import jax
import jax.numpy as jnp
import numpy as np
from jax import lax
from jax.experimental import pallas as pl
from jax.experimental.pallas import tpu as pltpu
from jax.sharding import PartitionSpec as P


EPS = 1e-06
THETA = 10000.0
BF = jnp.bfloat16
F32 = jnp.float32


END_ROWS = 8
SENT_ROWS = 16

VMEM = pl.BlockSpec(memory_space=pltpu.VMEM)


def inverses(size):
    powers = THETA ** (-np.arange(size // 2, dtype=np.float64) * 2.0 / size)
    return jnp.asarray(powers[None, :], F32)


def first_core():
    return lax.rem(lax.axis_index("sp"), 2) == 0


def reversed_bits(number, count):
    bits = count.bit_length() - 1
    return sum(((number >> i) & 1) << (bits - 1 - i) for i in range(bits))


def column_block(j, count):
    return lax.axis_index("tp") ^ jnp.where(first_core(), j, reversed_bits(j, count))


def turned(ref, head, size, cosine, sine):
    half = size // 2
    lower = ref[:, head * size : head * size + half].astype(F32)
    upper = ref[:, head * size + half : (head + 1) * size].astype(F32)
    return lower * cosine - upper * sine, upper * cosine + lower * sine


def triangle(count, lower):
    i = lax.broadcasted_iota(jnp.int32, (count, count), 0)
    j = lax.broadcasted_iota(jnp.int32, (count, count), 1)
    return i >= j if lower else i <= j


def contract(a, b, dims, precision=None):
    return lax.dot_general(
        a, b, (dims, ((), ())), preferred_element_type=F32, precision=precision
    )


def update_kernel(
    heads, key_a, key_b, value, inverse_a, inverse_b, rates,
    rot_a, rot_b, mine, theirs, decay, cos_a, sin_a, cos_b, sin_b,
):
    count = rates.shape[2]
    first = first_core()
    spot = lax.axis_index("sp") * count
    for inverse, cos, sin in ((inverse_a, cos_a, sin_a), (inverse_b, cos_b, sin_b)):
        spots = lax.broadcasted_iota(jnp.int32, cos.shape, 0) + spot
        angle = spots.astype(F32) * inverse[...]
        cos[...] = jnp.cos(angle)
        sin[...] = jnp.sin(angle)
    tri = triangle(count, True).astype(F32)
    sums = jnp.concatenate(
        [
            contract(tri, rates[group], ((1,), (1,)), lax.Precision.HIGHEST)
            for group in range(2)
        ],
        axis=1,
    )
    decay[...] = sums
    left = jnp.exp(sums[count - 1 : count, :] - sums)
    value_size = value.shape[1] // (2 * heads)
    row = 0
    for group, (key, rot, cos, sin) in enumerate(
        ((key_a, rot_a, cos_a, sin_a), (key_b, rot_b, cos_b, sin_b))
    ):
        size = key.shape[1] // heads
        half = size // 2
        for head in range(heads):
            column = group * heads + head
            values = value[:, column * value_size : (column + 1) * value_size]
            factor = left[:, column : column + 1]
            updates = []
            for part, turn in enumerate(turned(key, head, size, cos[...], sin[...])):
                keys = (turn * size ** (-0.5)).astype(BF)
                start = head * size + part * half
                rot[:, start : start + half] = keys
                carried = (keys.astype(F32) * factor).astype(BF)
                updates.append(contract(carried, values, ((0,), (0,))))
            mine[head, row : row + half, :] = jnp.where(first, updates[0], updates[1])
            theirs[head, row : row + half, :] = jnp.where(first, updates[1], updates[0])
        row += half
    lanes = mine.shape[2]
    which = lax.broadcasted_iota(jnp.int32, (END_ROWS, lanes), 0)
    for head in range(heads):
        pair = [
            jnp.broadcast_to(
                sums[count - 1 : count, column : column + 1], (END_ROWS, lanes)
            )
            for column in (head, heads + head)
        ]
        block = jnp.where(which == 0, pair[0], pair[1])
        mine[head, row : row + END_ROWS, :] = block
        theirs[head, row : row + END_ROWS, :] = block


def chip_kernel(half_a, mine, got, out):
    first = first_core()
    heads, height, lanes = mine.shape
    row = height - END_ROWS
    which = lax.broadcasted_iota(jnp.int32, (SENT_ROWS, lanes), 0)
    for head in range(heads):
        one, two = mine[head], got[head]
        before, after = jnp.where(first, one, two), jnp.where(first, two, one)
        begin = 0
        block = jnp.zeros((SENT_ROWS, lanes), F32)
        for group, end in enumerate((half_a, row)):
            last = after[row + group : row + group + 1, :]
            out[head, begin:end, :] = (
                jnp.exp(last) * before[begin:end, :] + after[begin:end, :]
            ).astype(BF)
            begin = end
            total = before[row + group : row + group + 1, :] + last
            for digit in range(3):
                part = total.astype(BF).astype(F32)
                total = total - part
                block = jnp.where(which == 3 * group + digit, part, block)
        out[head, row : row + SENT_ROWS, :] = block.astype(BF)


def state_kernel(half_a, count, *refs):
    arrived, (mine, got, out_mine, out_theirs) = refs[:count], refs[count:]
    first = first_core()
    heads, height, lanes = mine.shape
    row = height - END_ROWS
    for head in range(heads):
        begin = 0
        for group, end in enumerate((half_a, row)):
            span = slice(begin, end)
            state = arrived[0][head, span, :].astype(F32)
            passed = jnp.zeros((1, lanes), F32)
            for k in range(1, count):
                block = arrived[k - 1][head, row : row + SENT_ROWS, :].astype(F32)
                for digit in range(3):
                    at = 3 * group + digit
                    passed = passed + block[at : at + 1, :]
                state = state + jnp.exp(passed) * arrived[k][head, span, :].astype(F32)
            at = row + group
            update = jnp.where(first, mine[head, span, :], got[head, span, :])
            last = jnp.where(first, mine[head, at : at + 1, :], got[head, at : at + 1, :])
            later = jnp.exp(last) * state + update
            out_mine[head, span, :] = jnp.where(first, state, later).astype(BF)
            out_theirs[head, span, :] = jnp.where(first, later, state).astype(BF)
            begin = end


def norm_kernel(parts, others, *refs):
    own, refs = refs[0], refs[1:]
    moved, refs = refs[:others], refs[others:]
    residual, gain, refs = refs[:parts], refs[parts : 2 * parts], refs[2 * parts :]
    normed, mixed, stream = refs[0], refs[1:-1], refs[-1]
    width = own.shape[2]
    square = None
    for j in range(parts):
        total = own[j]
        for ref in moved:
            total = total + ref[j].astype(F32)
        rounded = total.astype(BF)
        mixed[j][...] = rounded
        row = residual[j][...].astype(F32) + rounded.astype(F32)
        stream[j] = row
        part = jnp.sum(row * row, axis=1, keepdims=True)
        square = part if square is None else square + part
    scale = lax.rsqrt(square / (parts * width) + EPS)
    for j in range(parts):
        begin = pl.multiple_of(column_block(j, parts) * width, width)
        normed[:, pl.ds(begin, width)] = (stream[j] * scale * gain[j][...]).astype(BF)


def within_kernel(
    heads, query_a, query_b, key_a, key_b, value, cos_a, sin_a, cos_b, sin_b,
    decay, rates, gates, gain, rot_a, rot_b, within, factor,
):
    count = decay.shape[0]
    lower = triangle(count, True)
    upper = triangle(count, False).astype(F32)
    value_size = value.shape[1] // (2 * heads)
    gate = gates[...].astype(F32)
    factor[...] = gain[...] * (gate / (1.0 + jnp.exp(-gate)))
    for group, (query, key, rot, cos, sin) in enumerate(
        ((query_a, key_a, rot_a, cos_a, sin_a), (query_b, key_b, rot_b, cos_b, sin_b))
    ):
        size = key.shape[1] // heads
        half = size // 2
        across = contract(rates[group], upper, ((1,), (0,)), lax.Precision.HIGHEST)
        for head in range(heads):
            column = group * heads + head
            start = head * size
            low, high = turned(query, head, size, cos[...], sin[...])
            rot[:, start : start + half] = low.astype(BF)
            rot[:, start + half : start + size] = high.astype(BF)
            scores = contract(
                rot[:, start : start + size], key[:, start : start + size], ((1,), (1,))
            )
            spread = decay[:, column : column + 1] - across[head : head + 1, :]
            weight = jnp.where(lower, jnp.exp(jnp.where(lower, spread, 0.0)), 0.0)
            place = slice(column * value_size, (column + 1) * value_size)
            within[:, place] = contract(
                (scores * weight).astype(BF), value[:, place], ((1,), (0,))
            )


def output_kernel(
    heads, query_a, query_b, within, decay, mine, got, factor, *outs
):
    held = outs[-1]
    first = first_core()
    value_size = within.shape[1] // (2 * heads)
    row = 0
    for group, query in enumerate((query_a, query_b)):
        size = query.shape[1] // heads
        half = size // 2
        for head in range(heads):
            column = group * heads + head
            one, two = mine[head, row : row + half, :], got[head, row : row + half, :]
            start = head * size
            cross = contract(
                query[:, start : start + half], jnp.where(first, one, two), ((1,), (0,))
            ) + contract(
                query[:, start + half : start + size], jnp.where(first, two, one), ((1,), (0,))
            )
            span = slice(column * value_size, (column + 1) * value_size)
            retained = within[:, span] + cross * jnp.exp(decay[:, column : column + 1])
            mean = jnp.mean(retained * retained, axis=1, keepdims=True)
            held[:, span] = retained * lax.rsqrt(mean + EPS) * factor[:, span]
        row += half
    for j, out in enumerate(outs[:-1]):
        piece = out.shape[0]
        begin = pl.multiple_of(column_block(j, len(outs) - 1) * piece, piece)
        out[...] = held[pl.ds(begin, piece), :].astype(BF)


def per_device(
    residual,
    query_small,
    key_narrow_group,
    query_large,
    key_large,
    values,
    gates,
    log_decay,
    head_gain,
    out_weight,
    norm_gain,
    routes,
    route_weight,
    expert_gate,
    expert_up,
    expert_down,
):
    S, T = lax.axis_size("sp"), lax.axis_size("tp")
    Z = S // 2
    s, t = lax.axis_index("sp"), lax.axis_index("tp")
    z, c = s // 2, s % 2
    first = c == 0
    rows = residual.shape[0]
    piece = rows // T
    heads = log_decay.shape[2]
    width = residual.shape[1]

    def swap(x):
        return lax.ppermute(x, "sp", [(a, a ^ 1) for a in range(S)])

    def zshift(x, k, wrap=True):
        if k == 0:
            return x
        pairs = [(a, a + 2 * k) for a in range(S)]
        pairs = [(a, b % S) for a, b in pairs if wrap or 0 <= b < S]
        return lax.ppermute(x, "sp", pairs)

    def across(x, j):
        if j == 0:
            return x
        pairs = []
        for a in range(S):
            far = j if a % 2 == 0 else reversed_bits(j, T)
            pairs += [(a * T + b, a * T + (b ^ far)) for b in range(T)]
        return lax.ppermute(x, ("sp", "tp"), pairs)

    bits = [1 << i for i in range(T.bit_length() - 1)]

    def crossed(x, i):
        pairs = []
        for a in range(S):
            bit = bits[i] if a % 2 == 0 else bits[len(bits) - 1 - i]
            pairs += [(a * T + b, a * T + (b ^ bit)) for b in range(T)]
        return lax.ppermute(x, ("sp", "tp"), pairs)

    def gathered(x):
        parts, number = [x], 0
        for i in range(len(bits)):
            new = []
            for part in parts:
                new.append(crossed(part, i))
                number += 1
            parts = parts + new
        return parts

    def pick(x, i):
        return lax.dynamic_index_in_dim(x, i, 0, keepdims=False)

    def by_xor(x, axis):
        for bit in bits:
            shape = x.shape
            split = x.reshape(shape[:axis] + (T // (2 * bit), 2, bit) + shape[axis + 1 :])
            flipped = jnp.flip(split, axis + 1)
            x = jnp.where((t // bit) % 2 == 1, flipped, split).reshape(shape)
        return x

    def by_core(x, axis, core_zero):
        shape = x.shape
        n = len(bits)
        split = x.reshape(shape[:axis] + (2,) * n + shape[axis + 1 :])
        order = list(range(split.ndim))
        order[axis : axis + n] = order[axis : axis + n][::-1]
        return jnp.where(core_zero, x, split.transpose(order).reshape(shape))

    def ordered(mine, other):
        return jnp.where(first, mine, other), jnp.where(first, other, mine)

    size_a, size_b = query_small.shape[1] // heads, query_large.shape[1] // heads
    value_rows = values.reshape(rows, -1)
    rates = log_decay.transpose(1, 2, 0)

    def after(values, *earlier):
        return lax.optimization_barrier((values, earlier))[0]

    half_a, half_b = size_a // 2, size_b // 2
    height, value_size = half_a + half_b, value_rows.shape[1] // (2 * heads)
    halves = (heads, height + END_ROWS, value_size)
    key_a, key_b, mine, theirs, decay, *tables = pl.pallas_call(
        functools.partial(update_kernel, heads),
        out_shape=(
            jax.ShapeDtypeStruct(key_narrow_group.shape, BF),
            jax.ShapeDtypeStruct(key_large.shape, BF),
            jax.ShapeDtypeStruct(halves, F32),
            jax.ShapeDtypeStruct(halves, F32),
            jax.ShapeDtypeStruct((rows, 2 * heads), F32),
            jax.ShapeDtypeStruct((rows, half_a), F32),
            jax.ShapeDtypeStruct((rows, half_a), F32),
            jax.ShapeDtypeStruct((rows, half_b), F32),
            jax.ShapeDtypeStruct((rows, half_b), F32),
        ),
        in_specs=[VMEM] * 6,
        out_specs=(VMEM,) * 9,
        name="update",
    )(key_narrow_group, key_large, value_rows, inverses(size_a), inverses(size_b), rates)

    got = swap(theirs)
    chip_update = pl.pallas_call(
        functools.partial(chip_kernel, half_a),
        out_shape=jax.ShapeDtypeStruct((heads, height + SENT_ROWS, value_size), BF),
        in_specs=[VMEM, VMEM],
        out_specs=VMEM,
        name="chip",
    )(mine, got)
    arrived = [zshift(chip_update, k, False) for k in range(1, Z)]

    turned_a, turned_b, within, factor = pl.pallas_call(
        functools.partial(within_kernel, heads),
        out_shape=(
            jax.ShapeDtypeStruct(query_small.shape, BF),
            jax.ShapeDtypeStruct(query_large.shape, BF),
            jax.ShapeDtypeStruct(value_rows.shape, F32),
            jax.ShapeDtypeStruct(value_rows.shape, F32),
        ),
        in_specs=[VMEM] * 13,
        out_specs=(VMEM,) * 4,
        name="within",
    )(
        query_small, query_large, key_a, key_b, value_rows, *tables, decay, rates,
        gates.reshape(rows, -1), head_gain.reshape(1, -1),
    )

    weight_own = gathered(after(out_weight, theirs))
    residual_in, gain_in = after((residual, norm_gain), chip_update, within)
    residual_pieces = residual_in.reshape(T, piece, width)
    residual_rows = [across(pick(residual_pieces, column_block(j, T)), j) for j in range(T)]
    gain_parts = [across(gain_in, j) for j in range(T)]

    experts = S
    capacity = 4 * rows // experts
    one_hot = (routes[:, :, None] == jnp.arange(experts, dtype=jnp.int32)).astype(jnp.int32)
    one_hot = one_hot.reshape(2 * rows, experts)
    before = jnp.cumsum(one_hot, axis=0) - one_hot
    slot_index = jnp.sum(before * one_hot, axis=1).reshape(rows, 2)
    info = jnp.concatenate(
        [routes.astype(F32), slot_index.astype(F32), route_weight, route_weight], axis=1
    )
    state_mine, state_theirs = pl.pallas_call(
        functools.partial(state_kernel, half_a, Z - 1),
        out_shape=(jax.ShapeDtypeStruct((heads, height, value_size), BF),) * 2,
        in_specs=[VMEM] * (Z + 1),
        out_specs=(VMEM, VMEM),
        name="state",
    )(*after(arrived, within), mine, got)
    state_got = swap(state_theirs)
    parts = pl.pallas_call(
        functools.partial(output_kernel, heads),
        out_shape=(jax.ShapeDtypeStruct((piece, value_rows.shape[1]), BF),) * T,
        in_specs=[VMEM] * 7,
        out_specs=(VMEM,) * T,
        scratch_shapes=[pltpu.VMEM(value_rows.shape, F32)],
        name="output",
    )(
        turned_a, turned_b, within, decay, state_mine, state_got, factor
    )

    depth = 2 * out_weight.shape[1]
    parts = [across(parts[j], j) for j in range(T)]
    weight_other = [swap(w) for w in after(weight_own, parts)]
    parts = by_core(jnp.stack(parts), 0, first)
    sent = [zshift(pick(parts, ((z + k) % Z) ^ t), k) for k in range(Z)]
    sent = jnp.concatenate(sent, axis=0)
    pairs = [
        ordered(sent[:, (i - 1) * (depth // 2) : i * (depth // 2)], sent[:, i * (depth // 2) : (i + 1) * (depth // 2)])
        for i in (1, 3)
    ]
    left_own = jnp.concatenate([pairs[0][0], pairs[1][0]], axis=1)
    left_other = jnp.concatenate([pairs[0][1], pairs[1][1]], axis=1)
    weight_other = [weight_other[reversed_bits(j, T)] for j in range(T)]
    products = [
        jnp.dot(left_own, weight_own[j].reshape(depth, width), preferred_element_type=F32)
        + jnp.dot(left_other, weight_other[j].reshape(depth, width), preferred_element_type=F32)
        for j in range(T)
    ]
    product = jnp.stack([p.reshape(Z, piece, width) for p in products], axis=1)
    outgoing = product.astype(BF)
    info = after(info, outgoing)
    info_pair = jnp.stack([info, swap(info)])
    infos = [zshift(info_pair, k) for k in range(Z)]
    moved = [zshift(outgoing[k], -k) for k in range(1, Z)]
    *normed, = pl.pallas_call(
        functools.partial(norm_kernel, T, Z - 1),
        out_shape=(jax.ShapeDtypeStruct((piece, T * width), BF),)
        + (jax.ShapeDtypeStruct((piece, width), BF),) * T,
        in_specs=[VMEM] * (Z + 2 * T),
        out_specs=(VMEM,) * (T + 1),
        scratch_shapes=[pltpu.VMEM((T, piece, width), F32)],
        name="norm",
    )(product[0], *moved, *residual_rows, *[g.reshape(1, -1) for g in gain_parts])
    normed, mixed = normed[0], normed[1:]

    own = s.astype(F32)
    slots = jnp.arange(capacity, dtype=jnp.int32).astype(F32)

    def slot_of(part):
        return jnp.where(
            part[..., 0] == own, part[..., 2], jnp.where(part[..., 1] == own, part[..., 3], -1.0)
        )

    def choose(part, core_zero, pieces_first):
        n = part.shape[0]
        part = by_xor(part.reshape(n, T, piece, part.shape[2]), 1)
        slot = slot_of(by_core(part, 1, core_zero))
        numbers = jnp.arange(n, dtype=jnp.int32)
        same = numbers[:, None] == numbers[None, :]
        hit = slots[None, :, None, None, None] == slot[None, None]
        hit = hit & same[:, None, :, None, None]
        if pieces_first:
            hit = hit.transpose(0, 1, 3, 2, 4)
        return hit.astype(BF).reshape(n * capacity, n * rows)

    def give(part, result):
        back = (slot_of(part)[:, :, None] == slots[None, None, :]).astype(BF)
        weight = jnp.where(
            part[..., 0] == own, part[..., 4], jnp.where(part[..., 1] == own, part[..., 5], 0.0)
        )
        picked = jnp.einsum("kts,ksd->ktd", back, result, preferred_element_type=F32)
        return weight[..., None] * picked

    w_gate, w_up, w_down = (expert_gate[0], expert_up[0], expert_down[0])
    even = [k for k in range(Z) if k % 2 == 0]
    odd = [k for k in range(Z) if k % 2 == 1]
    here = {k: zshift(normed, k) for k in even + odd}
    back = [across(mixed[j], j) for j in range(T)]
    mixed_back = by_xor(by_core(jnp.stack(back), 0, first), 0)
    stream = residual.astype(F32) + mixed_back.reshape(rows, width).astype(F32)

    def expert_rows(group, parts, pieces_first):
        block = jnp.concatenate(parts, axis=0)
        block_other = swap(block)
        near = jnp.stack([infos[k][0] for k in group])
        far = jnp.stack([infos[k][1] for k in group])
        choices = choose(near, first, pieces_first), choose(far, c == 1, pieces_first)
        taken = jnp.concatenate(
            [
                jnp.dot(choices[0], block, preferred_element_type=F32),
                jnp.dot(choices[1], block_other, preferred_element_type=F32),
            ],
            axis=0,
        ).astype(BF)
        gate_part = jnp.dot(taken, w_gate, preferred_element_type=F32)
        up_part = jnp.dot(taken, w_up, preferred_element_type=F32)
        return (jax.nn.silu(gate_part) * up_part).astype(BF), near, far

    def expert_sums(group, parts, near, far):
        n = len(group)
        hidden = by_xor(by_core(jnp.stack(parts), 0, first), 0)
        hidden = hidden.transpose(1, 0, 2).reshape(2 * n * capacity, -1)
        result = jnp.dot(hidden, w_down, preferred_element_type=F32).astype(BF)
        result = result.reshape(2, n, capacity, width)
        far_part = swap(give(far, result[1]).astype(BF)).astype(F32)
        return give(near, result[0]) + far_part

    parts_even = [p for k in even for p in gathered(here[k])]
    joined = jnp.concatenate([here[k] for k in odd], axis=0)
    parts_odd = gathered(joined)
    hidden_even, near_even, far_even = expert_rows(even, parts_even, False)
    hidden_odd, near_odd, far_odd = expert_rows(odd, after(parts_odd, hidden_even), True)
    gathered_even = gathered(hidden_even)
    sums_even = expert_sums(even, after(gathered_even, hidden_odd), near_even, far_even)
    gathered_odd = gathered(hidden_odd)
    sums_odd = expert_sums(odd, after(gathered_odd, sums_even), near_odd, far_odd)
    routed = sums_even[0]
    for sums, group in ((sums_even, even), (sums_odd, odd)):
        for i, k in enumerate(group):
            if k > 0:
                routed = routed + zshift(sums[i].astype(BF), -k).astype(F32)
    return (stream + routed).astype(BF)


def solution(mesh):
    placed = (
        P("sp", "tp"),
        P("sp", "tp"),
        P("sp", "tp"),
        P("sp", "tp"),
        P("sp", "tp"),
        P("sp", None, "tp"),
        P("sp", None, "tp"),
        P("sp", None, "tp"),
        P(None, "tp"),
        P(None, "sp", "tp"),
        P("tp"),
        P("sp", None),
        P("sp", None),
        P("sp", None, "tp"),
        P("sp", None, "tp"),
        P("sp", None, "tp"),
    )

    return jax.shard_map(
        per_device, mesh=mesh, in_specs=placed, out_specs=P("sp", "tp"), check_vma=False
    )
```

profile of v0, /device:TPU:0, one launch (start us, length us, event | category | flops | bytes accessed | tf_op | source)
XLA Modules:
  0.0 281.4 jit_solution(6145301307877967628)
XLA Ops:
  1.7 3.7 %update.1 = (bf16[128,512]{1,0:T(8,128)(2,1)}, bf16[128,1024]{1,0:T(8,128)(2,1)}, f32[4,200,128]{2,1,0:T(8,128)}, f32[4,200,128]{2,1,0:T(8,128)}, f32[128,8]{1,0...) custom-call(bf16[128,512]{1,0:T(8,128)(2,1)} %key_a.1, ...), custom_call_target="tpu_custom_call" | custom-call | tf_op jit(solution)/shard_map/update/pallas_call | solution.py:352
  5.4 3.0 %collective-permute-start.11 = (bf16[2,256,1024]{2,1,0:T(8,128)(2,1)}, bf16[2,256,1024]{2,1,0:T(8,128)(2,1)S(1)}, u32[]{:S(2)}, u32[]{:S(2)}) collective-permute-start(bf16[2,256,1024]{2,1,0:T(8,128)(2,1)} %param.27), channel_id=1, source_target_pairs={{0,1},{1,0},{2,3},{3,2},{4,6},{5,7},{6,4},{7,5},{8,9},{9,8},{10,11... | collective-permute-start | bytes 3145736 | tf_op jit(solution)/shard_map/ppermute | solution.py:308
  9.9 22.2 %collective-permute-done.11 = bf16[2,256,1024]{2,1,0:T(8,128)(2,1)S(1)} collective-permute-done((bf16[2,256,1024]{2,1,0:T(8,128)(2,1)}, bf16[2,256,1024]{2,1,0:T(8,128)(2,1)S(1)}, u32[]{:S(2)}, u32[]{:S(2)}) %collective-permute-start.11) | collective-permute-done | bytes 1048608 | tf_op jit(solution)/shard_map/ppermute | solution.py:308
  43.4 3.6 %collective-permute-start.1 = (bf16[4,208,128]{2,1,0:T(8,128)(2,1)}, bf16[4,208,128]{2,1,0:T(8,128)(2,1)S(1)}, u32[]{:S(2)}, u32[]{:S(2)}) collective-permute-start(bf16[4,208,128]{2,1,0:T(8,128)(2,1)} %chip.1), channel_id=1, source_target_pairs={{0,8},{4,12},{8,16},{12,20},{16,24},{20,28},{1,9},{5,13},{9,17},{1... | collective-permute-start | bytes 638984 | tf_op jit(solution)/shard_map/ppermute | solution.py:290
  47.0 5.2 %collective-permute-start.2 = (bf16[4,208,128]{2,1,0:T(8,128)(2,1)}, bf16[4,208,128]{2,1,0:T(8,128)(2,1)}, u32[]{:S(2)}, u32[]{:S(2)}) collective-permute-start(bf16[4,208,128]{2,1,0:T(8,128)(2,1)} %chip.1), channel_id=1, source_target_pairs={{0,16},{4,20},{8,24},{12,28},{1,17},{5,21},{9,25},{13,29},{2,18},{... | collective-permute-start | bytes 638984 | tf_op jit(solution)/shard_map/ppermute | solution.py:290
  58.7 3.7 %within.1 = (bf16[128,512]{1,0:T(8,128)(2,1)}, bf16[128,1024]{1,0:T(8,128)(2,1)}, f32[128,1024]{1,0:T(8,128)}, f32[128,1024]{1,0:T(8,128)}) custom-call(bf16[128,512]{1,0:T(8,128)(2,1)} %query_a.1, bf16[128,1024]{1,0:T(8,128)(2,1)} %query_b.1, bf16[128,512]{1,0:T(8,128)(2,1)} %get-tuple-element.52.key_a, bf16[128,1024]{1,0:T(8,128)(2,1)} %get-tuple-element.53.key_b, ...), custom_call_target="tpu_custom_call" | custom-call | tf_op jit(solution)/shard_map/within/pallas_call | solution.py:380
  63.1 2.3 state.1
  67.7 3.0 %output.1 = (bf16[32,1024]{1,0:T(8,128)(2,1)}, bf16[32,1024]{1,0:T(8,128)(2,1)}, bf16[32,1024]{1,0:T(8,128)(2,1)}, bf16[32,1024]{1,0:T(8,128)(2,1)}) custom-call(bf16[128,512]{1,0:T(8,128)(2,1)} %get-tuple-element.59.query_a, bf16[128,1024]{1,0:T(8,128)(2,1)} %get-tuple-element.60.query_b, f32[128,1024]{1,0:T(8,128)} %get-tuple-element.61.within, ...), custom_call_target="tpu_custom_call" | custom-call | tf_op jit(solution)/shard_map/output/pallas_call | solution.py:419
  70.8 2.4 collective-permute-start.5
  76.0 2.4 collective-permute-done.6
  81.5 4.0 %collective-permute-start.10 = (bf16[32,1024]{1,0:T(8,128)(2,1)S(1)}, bf16[32,1024]{1,0:T(8,128)(2,1)S(1)}, u32[]{:S(2)}, u32[]{:S(2)}) collective-permute-start(bf16[32,1024]{1,0:T(8,128)(2,1)S(1)} %get-tuple-element.117), channel_id=1, source_target_pairs={{0,24},{4,28},{8,0},{12,4},{16,8},{20,12},{24,16},{28,20},{1,25},{... | collective-permute-start | bytes 196616 | tf_op jit(solution)/shard_map/ppermute | solution.py:290
  92.9 2.7 collective-permute-start.26
  105.1 5.5 %collective-permute-done.43 = f32[2,128,8]{1,2,0:T(8,128)S(1)} collective-permute-done((f32[2,128,8]{1,2,0:T(8,128)S(1)}, f32[2,128,8]{1,2,0:T(8,128)S(1)}, u32[]{:S(2)}, u32[]{:S(2)}) %collective-permute-start.43) | collective-permute-done | bytes 8224 | tf_op jit(solution)/shard_map/ppermute | solution.py:290
  111.1 4.1 %collective-permute-done.31 = f32[2,128,8]{1,2,0:T(8,128)S(1)} collective-permute-done((f32[2,128,8]{1,2,0:T(8,128)S(1)}, f32[2,128,8]{1,2,0:T(8,128)S(1)}, u32[]{:S(2)}, u32[]{:S(2)}) %collective-permute-start.31) | collective-permute-done | bytes 8224 | tf_op jit(solution)/shard_map/ppermute | solution.py:290
  125.4 12.0 %collective-permute-done.19.refs_2_ = bf16[4,32,1024]{2,1,0:T(8,128)(2,1)S(1)} collective-permute-done((bf16[4,32,1024]{2,1,0:T(8,128)(2,1)S(1)}, bf16[4,32,1024]{2,1,0:T(8,128)(2,1)S(1)}, u32[]{:S(2)}, u32[]{:S(2)}) %collective-permute-start.19) | collective-permute-done | bytes 262176 | tf_op jit(solution)/shard_map/ppermute | solution.py:290
  138.2 2.4 norm.1
  142.7 2.5 collective-permute-start.35
  146.2 16.3 %collective-permute-done.35 = bf16[32,4096]{1,0:T(8,128)(2,1)S(1)} collective-permute-done((bf16[32,4096]{1,0:T(8,128)(2,1)}, bf16[32,4096]{1,0:T(8,128)(2,1)S(1)}, u32[]{:S(2)}, u32[]{:S(2)}) %collective-permute-start.35) | collective-permute-done | bytes 262176 | tf_op jit(solution)/shard_map/ppermute | solution.py:290
  165.9 7.5 %collective-permute-done.34 = bf16[32,4096]{1,0:T(8,128)(2,1)S(1)} collective-permute-done((bf16[32,4096]{1,0:T(8,128)(2,1)S(1)}, bf16[32,4096]{1,0:T(8,128)(2,1)S(1)}, u32[]{:S(2)}, u32[]{:S(2)}) %collective-permute-start.34) | collective-permute-done | bytes 262176 | tf_op jit(solution)/shard_map/ppermute | solution.py:308
  175.2 4.7 %collective-permute-done.38 = bf16[32,4096]{1,0:T(8,128)(2,1)S(1)} collective-permute-done((bf16[32,4096]{1,0:T(8,128)(2,1)S(1)}, bf16[32,4096]{1,0:T(8,128)(2,1)S(1)}, u32[]{:S(2)}, u32[]{:S(2)}) %collective-permute-start.38) | collective-permute-done | bytes 262176 | tf_op jit(solution)/shard_map/ppermute | solution.py:308
  180.2 8.6 %collective-permute-done.46 = bf16[32,4096]{1,0:T(8,128)(2,1)S(1)} collective-permute-done((bf16[32,4096]{1,0:T(8,128)(2,1)S(1)}, bf16[32,4096]{1,0:T(8,128)(2,1)S(1)}, u32[]{:S(2)}, u32[]{:S(2)}) %collective-permute-start.46) | collective-permute-done | bytes 262176 | tf_op jit(solution)/shard_map/ppermute | solution.py:290
  192.0 10.5 %collective-permute-done.47 = bf16[64,4096]{1,0:T(8,128)(2,1)S(1)} collective-permute-done((bf16[64,4096]{1,0:T(8,128)(2,1)S(1)}, bf16[64,4096]{1,0:T(8,128)(2,1)S(1)}, u32[]{:S(2)}, u32[]{:S(2)}) %collective-permute-start.47) | collective-permute-done | bytes 524320 | tf_op jit(solution)/shard_map/ppermute | solution.py:308
  202.5 2.8 collective-permute-start.49
  216.4 5.4 %collective-permute-done.40 = bf16[256,512]{1,0:T(8,128)(2,1)S(1)} collective-permute-done((bf16[256,512]{1,0:T(8,128)(2,1)S(1)}, bf16[256,512]{1,0:T(8,128)(2,1)S(1)}, u32[]{:S(2)}, u32[]{:S(2)}) %collective-permute-start.40) | collective-permute-done | bytes 262176 | tf_op jit(solution)/shard_map/ppermute | solution.py:308
  221.8 2.8 collective-permute-start.42
  231.6 3.5 %fusion.14 = bf16[256,1024]{1,0:T(8,128)(2,1)S(1)} fusion(bf16[256,2048]{0,1:T(8,128)(2,1)S(1)} %bitcast.261, bf16[1,2048,1024]{2,1,0:T(8,128)(2,1)} %param.33), kind=kOutput, calls=%fused_computation.29 | convolution fusion | flops 1074003968 | bytes 5767168 | tf_op jit(solution)/shard_map/dot_general | solution.py:522
  239.8 3.7 %collective-permute-done.53 = bf16[256,512]{1,0:T(8,128)(2,1)S(1)} collective-permute-done((bf16[256,512]{1,0:T(8,128)(2,1)S(1)}, bf16[256,512]{1,0:T(8,128)(2,1)S(1)}, u32[]{:S(2)}, u32[]{:S(2)}) %collective-permute-start.53) | collective-permute-done | bytes 262176 | tf_op jit(solution)/shard_map/ppermute | solution.py:308
  246.0 3.9 %collective-permute-done.54 = bf16[256,512]{1,0:T(8,128)(2,1)S(1)} collective-permute-done((bf16[256,512]{1,0:T(8,128)(2,1)S(1)}, bf16[256,512]{1,0:T(8,128)(2,1)S(1)}, u32[]{:S(2)}, u32[]{:S(2)}) %collective-permute-start.54) | collective-permute-done | bytes 262176 | tf_op jit(solution)/shard_map/ppermute | solution.py:308
  249.9 2.8 collective-permute-done.55
  253.9 3.5 %fusion.17 = bf16[256,1024]{1,0:T(8,128)(2,1)S(1)} fusion(bf16[256,2048]{0,1:T(8,128)(2,1)S(1)} %bitcast.262, bf16[1,2048,1024]{2,1,0:T(8,128)(2,1)} %param.33), kind=kOutput, calls=%fused_computation.30 | convolution fusion | flops 1074003968 | bytes 5767168 | tf_op jit(solution)/shard_map/dot_general | solution.py:522
  261.2 3.0 %collective-permute-start.57 = (bf16[128,1024]{1,0:T(8,128)(2,1)S(1)}, bf16[128,1024]{1,0:T(8,128)(2,1)S(1)}, u32[]{:S(2)}, u32[]{:S(2)}) collective-permute-start(bf16[128,1024]{1,0:T(8,128)(2,1)S(1)} %get-tuple-element.102), channel_id=1, source_target_pairs={{0,24},{4,28},{8,0},{12,4},{16,8},{20,12},{24,16},{28,20},{1,25},{... | collective-permute-start | bytes 786440 | tf_op jit(solution)/shard_map/ppermute | solution.py:290
  264.3 14.1 %collective-permute-done.52 = bf16[128,1024]{1,0:T(8,128)(2,1)S(1)} collective-permute-done((bf16[128,1024]{1,0:T(8,128)(2,1)S(1)}, bf16[128,1024]{1,0:T(8,128)(2,1)S(1)}, u32[]{:S(2)}, u32[]{:S(2)}) %collective-permute-start.52) | collective-permute-done | bytes 262176 | tf_op jit(solution)/shard_map/ppermute | solution.py:290
  (288 shorter events, 102.5 us)
Async XLA Ops:
  5.4 26.7 %collective-permute-start.11 = (bf16[2,256,1024]{2,1,0:T(8,128)(2,1)}, bf16[2,256,1024]{2,1,0:T(8,128)(2,1)S(1)}, u32[]{:S(2)}, u32[]{:S(2)}) collective-permute-start(bf16[2,256,1024]{2,1,0:T(8,128)(2,1)} %param.27), channel_id=1, source_target_pairs={{0,1},{1,0},{2,3},{3,2},{4,6},{5,7},{6,4},{7,5},{8,9},{9,8},{10,11... | collective-permute-start | bytes 3145736 | tf_op jit(solution)/shard_map/ppermute | solution.py:308
  8.4 32.3 %collective-permute-start = (f32[4,200,128]{2,1,0:T(8,128)}, f32[4,200,128]{2,1,0:T(8,128)S(1)}, u32[]{:S(2)}, u32[]{:S(2)}) collective-permute-start(f32[4,200,128]{2,1,0:T(8,128)} %get-tuple-element.63), channel_id=1, source_target_pairs={{0,4},{4,0},{8,12},{12,8},{16,20},{20,16},{24,28},{28,24},{1,5},{5... | collective-permute-start | bytes 1228808 | tf_op jit(solution)/shard_map/ppermute | solution.py:283
  8.4 71.6 %collective-permute-start.12 = (bf16[2,256,1024]{2,1,0:T(8,128)(2,1)}, bf16[2,256,1024]{2,1,0:T(8,128)(2,1)S(1)}, u32[]{:S(2)}, u32[]{:S(2)}) collective-permute-start(bf16[2,256,1024]{2,1,0:T(8,128)(2,1)} %param.27), channel_id=1, source_target_pairs={{0,2},{1,3},{2,0},{3,1},{4,5},{5,4},{6,7},{7,6},{8,10},{9,11},{10,... | collective-permute-start | bytes 3145736 | tf_op jit(solution)/shard_map/ppermute | solution.py:308
  32.1 47.8 %collective-permute-start.13 = (bf16[2,256,1024]{2,1,0:T(8,128)(2,1)S(1)}, bf16[2,256,1024]{2,1,0:T(8,128)(2,1)S(1)}, u32[]{:S(2)}, u32[]{:S(2)}) collective-permute-start(bf16[2,256,1024]{2,1,0:T(8,128)(2,1)S(1)} %collective-permute-done.11), channel_id=1, source_target_pairs={{0,2},{1,3},{2,0},{3,1},{4,5},{5,4},{6,7},{7,6},{8,10},{9,11},{10,... | collective-permute-start | bytes 3145736 | tf_op jit(solution)/shard_map/ppermute | solution.py:308
  43.4 19.0 %collective-permute-start.1 = (bf16[4,208,128]{2,1,0:T(8,128)(2,1)}, bf16[4,208,128]{2,1,0:T(8,128)(2,1)S(1)}, u32[]{:S(2)}, u32[]{:S(2)}) collective-permute-start(bf16[4,208,128]{2,1,0:T(8,128)(2,1)} %chip.1), channel_id=1, source_target_pairs={{0,8},{4,12},{8,16},{12,20},{16,24},{20,28},{1,9},{5,13},{9,17},{1... | collective-permute-start | bytes 638984 | tf_op jit(solution)/shard_map/ppermute | solution.py:290
  47.0 15.4 %collective-permute-start.2 = (bf16[4,208,128]{2,1,0:T(8,128)(2,1)}, bf16[4,208,128]{2,1,0:T(8,128)(2,1)}, u32[]{:S(2)}, u32[]{:S(2)}) collective-permute-start(bf16[4,208,128]{2,1,0:T(8,128)(2,1)} %chip.1), channel_id=1, source_target_pairs={{0,16},{4,20},{8,24},{12,28},{1,17},{5,21},{9,25},{13,29},{2,18},{... | collective-permute-start | bytes 638984 | tf_op jit(solution)/shard_map/ppermute | solution.py:290
  52.2 10.2 %collective-permute-start.3 = (bf16[4,208,128]{2,1,0:T(8,128)(2,1)}, bf16[4,208,128]{2,1,0:T(8,128)(2,1)}, u32[]{:S(2)}, u32[]{:S(2)}) collective-permute-start(bf16[4,208,128]{2,1,0:T(8,128)(2,1)} %chip.1), channel_id=1, source_target_pairs={{0,24},{4,28},{1,25},{5,29},{2,26},{6,30},{3,27},{7,31}} | collective-permute-start | bytes 638984 | tf_op jit(solution)/shard_map/ppermute | solution.py:290
  80.0 13.0 %collective-permute-start.17 = (bf16[2,256,1024]{2,1,0:T(8,128)(2,1)S(1)}, bf16[2,256,1024]{2,1,0:T(8,128)(2,1)S(1)}, u32[]{:S(2)}, u32[]{:S(2)}) collective-permute-start(bf16[2,256,1024]{2,1,0:T(8,128)(2,1)S(1)} %collective-permute-done.13), channel_id=1, source_target_pairs={{0,4},{4,0},{8,12},{12,8},{16,20},{20,16},{24,28},{28,24},{1,5},{5... | collective-permute-start | bytes 3145736 | tf_op jit(solution)/shard_map/ppermute | solution.py:283
  80.9 15.0 %collective-permute-start.16 = (bf16[2,256,1024]{2,1,0:T(8,128)(2,1)S(1)}, bf16[2,256,1024]{2,1,0:T(8,128)(2,1)S(1)}, u32[]{:S(2)}, u32[]{:S(2)}) collective-permute-start(bf16[2,256,1024]{2,1,0:T(8,128)(2,1)S(1)} %collective-permute-done.11), channel_id=1, source_target_pairs={{0,4},{4,0},{8,12},{12,8},{16,20},{20,16},{24,28},{28,24},{1,5},{5... | collective-permute-start | bytes 3145736 | tf_op jit(solution)/shard_map/ppermute | solution.py:283
  88.0 29.9 %collective-permute-start.24 = (f32[1024]{0:T(1024)S(1)}, f32[1024]{0:T(1024)S(1)}, u32[]{:S(2)}, u32[]{:S(2)}) collective-permute-start(f32[1024]{0:T(1024)S(1)} %copy-done.15), channel_id=1, source_target_pairs={{0,1},{1,0},{2,3},{3,2},{4,6},{5,7},{6,4},{7,5},{8,9},{9,8},{10,11... | collective-permute-start | bytes 12296 | tf_op jit(solution)/shard_map/ppermute | solution.py:299
  92.0 26.0 %collective-permute-start.25 = (f32[1024]{0:T(1024)S(1)}, f32[1024]{0:T(1024)S(1)}, u32[]{:S(2)}, u32[]{:S(2)}) collective-permute-start(f32[1024]{0:T(1024)S(1)} %copy-done.15), channel_id=1, source_target_pairs={{0,2},{1,3},{2,0},{3,1},{4,5},{5,4},{6,7},{7,6},{8,10},{9,11},{10,... | collective-permute-start | bytes 12296 | tf_op jit(solution)/shard_map/ppermute | solution.py:299
  92.9 25.6 %collective-permute-start.26 = (f32[1024]{0:T(1024)S(1)}, f32[1024]{0:T(1024)S(1)}, u32[]{:S(2)}, u32[]{:S(2)}) collective-permute-start(f32[1024]{0:T(1024)S(1)} %copy-done.15), channel_id=1, source_target_pairs={{0,3},{1,2},{2,1},{3,0},{4,7},{5,6},{6,5},{7,4},{8,11},{9,10},{10,... | collective-permute-start | bytes 12296 | tf_op jit(solution)/shard_map/ppermute | solution.py:299
  95.9 24.2 %collective-permute-start.21 = (bf16[32,1024]{1,0:T(8,128)(2,1)S(1)}, bf16[32,1024]{1,0:T(8,128)(2,1)S(1)}, u32[]{:S(2)}, u32[]{:S(2)}) collective-permute-start(bf16[32,1024]{1,0:T(8,128)(2,1)S(1)} %get-tuple-element.110), channel_id=1, source_target_pairs={{0,1},{1,0},{2,3},{3,2},{4,6},{5,7},{6,4},{7,5},{8,9},{9,8},{10,11... | collective-permute-start | bytes 196616 | tf_op jit(solution)/shard_map/ppermute | solution.py:299
  117.9 19.5 %collective-permute-start.19 = (bf16[4,32,1024]{2,1,0:T(8,128)(2,1)S(1)}, bf16[4,32,1024]{2,1,0:T(8,128)(2,1)S(1)}, u32[]{:S(2)}, u32[]{:S(2)}) collective-permute-start(bf16[4,32,1024]{2,1,0:T(8,128)(2,1)S(1)} %get-tuple-element.100), channel_id=1, source_target_pairs={{0,16},{4,20},{8,24},{12,28},{16,0},{20,4},{24,8},{28,12},{1,17},{... | collective-permute-start | bytes 786440 | tf_op jit(solution)/shard_map/ppermute | solution.py:290
  118.0 19.4 %collective-permute-start.20 = (bf16[4,32,1024]{2,1,0:T(8,128)(2,1)S(1)}, bf16[4,32,1024]{2,1,0:T(8,128)(2,1)S(1)}, u32[]{:S(2)}, u32[]{:S(2)}) collective-permute-start(bf16[4,32,1024]{2,1,0:T(8,128)(2,1)S(1)} %get-tuple-element.99), channel_id=1, source_target_pairs={{0,8},{4,12},{8,16},{12,20},{16,24},{20,28},{24,0},{28,4},{1,9},{5... | collective-permute-start | bytes 786440 | tf_op jit(solution)/shard_map/ppermute | solution.py:290
  140.6 23.9 %collective-permute-start.32 = (bf16[32,4096]{1,0:T(8,128)(2,1)}, bf16[32,4096]{1,0:T(8,128)(2,1)S(1)}, u32[]{:S(2)}, u32[]{:S(2)}) collective-permute-start(bf16[32,4096]{1,0:T(8,128)(2,1)} %get-tuple-element.86), channel_id=1, source_target_pairs={{0,1},{1,0},{2,3},{3,2},{4,6},{5,7},{6,4},{7,5},{8,9},{9,8},{10,11... | collective-permute-start | bytes 786440 | tf_op jit(solution)/shard_map/ppermute | solution.py:308
  142.3 23.5 %collective-permute-start.33 = (bf16[32,4096]{1,0:T(8,128)(2,1)}, bf16[32,4096]{1,0:T(8,128)(2,1)S(1)}, u32[]{:S(2)}, u32[]{:S(2)}) collective-permute-start(bf16[32,4096]{1,0:T(8,128)(2,1)} %get-tuple-element.86), channel_id=1, source_target_pairs={{0,2},{1,3},{2,0},{3,1},{4,5},{5,4},{6,7},{7,6},{8,10},{9,11},{10,... | collective-permute-start | bytes 786440 | tf_op jit(solution)/shard_map/ppermute | solution.py:308
  142.7 19.8 %collective-permute-start.35 = (bf16[32,4096]{1,0:T(8,128)(2,1)}, bf16[32,4096]{1,0:T(8,128)(2,1)S(1)}, u32[]{:S(2)}, u32[]{:S(2)}) collective-permute-start(bf16[32,4096]{1,0:T(8,128)(2,1)} %get-tuple-element.86), channel_id=1, source_target_pairs={{0,16},{4,20},{8,24},{12,28},{16,0},{20,4},{24,8},{28,12},{1,17},{... | collective-permute-start | bytes 786440 | tf_op jit(solution)/shard_map/ppermute | solution.py:290
  145.2 35.0 %collective-permute-start.45 = (bf16[32,4096]{1,0:T(8,128)(2,1)}, bf16[32,4096]{1,0:T(8,128)(2,1)S(1)}, u32[]{:S(2)}, u32[]{:S(2)}) collective-permute-start(bf16[32,4096]{1,0:T(8,128)(2,1)} %get-tuple-element.86), channel_id=1, source_target_pairs={{0,8},{4,12},{8,16},{12,20},{16,24},{20,28},{24,0},{28,4},{1,9},{5... | collective-permute-start | bytes 786440 | tf_op jit(solution)/shard_map/ppermute | solution.py:290
  162.5 11.0 %collective-permute-start.36 = (bf16[32,4096]{1,0:T(8,128)(2,1)S(1)}, bf16[32,4096]{1,0:T(8,128)(2,1)S(1)}, u32[]{:S(2)}, u32[]{:S(2)}) collective-permute-start(bf16[32,4096]{1,0:T(8,128)(2,1)S(1)} %collective-permute-done.35), channel_id=1, source_target_pairs={{0,1},{1,0},{2,3},{3,2},{4,6},{5,7},{6,4},{7,5},{8,9},{9,8},{10,11... | collective-permute-start | bytes 786440 | tf_op jit(solution)/shard_map/ppermute | solution.py:308
  163.8 11.4 %collective-permute-start.37 = (bf16[32,4096]{1,0:T(8,128)(2,1)S(1)}, bf16[32,4096]{1,0:T(8,128)(2,1)S(1)}, u32[]{:S(2)}, u32[]{:S(2)}) collective-permute-start(bf16[32,4096]{1,0:T(8,128)(2,1)S(1)} %collective-permute-done.35), channel_id=1, source_target_pairs={{0,2},{1,3},{2,0},{3,1},{4,5},{5,4},{6,7},{7,6},{8,10},{9,11},{10,... | collective-permute-start | bytes 786440 | tf_op jit(solution)/shard_map/ppermute | solution.py:308
  179.9 25.9 %collective-permute-start.39 = (bf16[256,4096]{1,0:T(8,128)(2,1)S(1)}, bf16[256,4096]{1,0:T(8,128)(2,1)}, u32[]{:S(2)}, u32[]{:S(2)}) collective-permute-start(bf16[256,4096]{1,0:T(8,128)(2,1)S(1)} %constant_dynamic-update-slice_fusion.2), channel_id=1, source_target_pairs={{0,4},{4,0},{8,12},{12,8},{16,20},{20,16},{24,28},{28,24},{1,5},{5... | collective-permute-start | bytes 6291464 | tf_op jit(solution)/shard_map/ppermute | solution.py:283
  188.8 13.7 %collective-permute-start.47 = (bf16[64,4096]{1,0:T(8,128)(2,1)S(1)}, bf16[64,4096]{1,0:T(8,128)(2,1)S(1)}, u32[]{:S(2)}, u32[]{:S(2)}) collective-permute-start(bf16[64,4096]{1,0:T(8,128)(2,1)S(1)} %constant_dynamic-update-slice_fusion.10), channel_id=1, source_target_pairs={{0,1},{1,0},{2,3},{3,2},{4,6},{5,7},{6,4},{7,5},{8,9},{9,8},{10,11... | collective-permute-start | bytes 1572872 | tf_op jit(solution)/shard_map/ppermute | solution.py:308
  191.2 20.4 %collective-permute-start.48 = (bf16[64,4096]{1,0:T(8,128)(2,1)S(1)}, bf16[64,4096]{1,0:T(8,128)(2,1)S(1)}, u32[]{:S(2)}, u32[]{:S(2)}) collective-permute-start(bf16[64,4096]{1,0:T(8,128)(2,1)S(1)} %constant_dynamic-update-slice_fusion.10), channel_id=1, source_target_pairs={{0,2},{1,3},{2,0},{3,1},{4,5},{5,4},{6,7},{7,6},{8,10},{9,11},{10,... | collective-permute-start | bytes 1572872 | tf_op jit(solution)/shard_map/ppermute | solution.py:308
  212.7 11.9 %collective-permute-start.50 = (bf16[256,4096]{1,0:T(8,128)(2,1)S(1)}, bf16[256,4096]{1,0:T(8,128)(2,1)}, u32[]{:S(2)}, u32[]{:S(2)}) collective-permute-start(bf16[256,4096]{1,0:T(8,128)(2,1)S(1)} %constant_dynamic-update-slice_fusion.12), channel_id=1, source_target_pairs={{0,4},{4,0},{8,12},{12,8},{16,20},{20,16},{24,28},{28,24},{1,5},{5... | collective-permute-start | bytes 6291464 | tf_op jit(solution)/shard_map/ppermute | solution.py:283
  215.2 14.9 %collective-permute-start.41 = (bf16[256,512]{1,0:T(8,128)(2,1)S(1)}, bf16[256,512]{1,0:T(8,128)(2,1)S(1)}, u32[]{:S(2)}, u32[]{:S(2)}) collective-permute-start(bf16[256,512]{1,0:T(8,128)(2,1)S(1)} %fusion.29), channel_id=1, source_target_pairs={{0,2},{1,3},{2,0},{3,1},{4,5},{5,4},{6,7},{7,6},{8,10},{9,11},{10,... | collective-permute-start | bytes 786440 | tf_op jit(solution)/shard_map/ppermute | solution.py:308
  236.2 21.7 %collective-permute-start.29 = (bf16[32,1024]{1,0:T(8,128)(2,1)}, bf16[32,1024]{1,0:T(8,128)(2,1)S(1)}, u32[]{:S(2)}, u32[]{:S(2)}) collective-permute-start(bf16[32,1024]{1,0:T(8,128)(2,1)} %get-tuple-element.84), channel_id=1, source_target_pairs={{0,3},{1,2},{2,1},{3,0},{4,7},{5,6},{6,5},{7,4},{8,11},{9,10},{10,... | collective-permute-start | bytes 196616 | tf_op jit(solution)/shard_map/ppermute | solution.py:299
  238.1 19.9 %collective-permute-start.28 = (bf16[32,1024]{1,0:T(8,128)(2,1)S(1)}, bf16[32,1024]{1,0:T(8,128)(2,1)S(1)}, u32[]{:S(2)}, u32[]{:S(2)}) collective-permute-start(bf16[32,1024]{1,0:T(8,128)(2,1)S(1)} %copy-done.27), channel_id=1, source_target_pairs={{0,2},{1,3},{2,0},{3,1},{4,5},{5,4},{6,7},{7,6},{8,10},{9,11},{10,... | collective-permute-start | bytes 196616 | tf_op jit(solution)/shard_map/ppermute | solution.py:299
  239.3 18.7 %collective-permute-start.27 = (bf16[32,1024]{1,0:T(8,128)(2,1)S(1)}, bf16[32,1024]{1,0:T(8,128)(2,1)S(1)}, u32[]{:S(2)}, u32[]{:S(2)}) collective-permute-start(bf16[32,1024]{1,0:T(8,128)(2,1)S(1)} %copy-done.26), channel_id=1, source_target_pairs={{0,1},{1,0},{2,3},{3,2},{4,6},{5,7},{6,4},{7,5},{8,9},{9,8},{10,11... | collective-permute-start | bytes 196616 | tf_op jit(solution)/shard_map/ppermute | solution.py:299
  258.1 20.3 %collective-permute-start.52 = (bf16[128,1024]{1,0:T(8,128)(2,1)S(1)}, bf16[128,1024]{1,0:T(8,128)(2,1)S(1)}, u32[]{:S(2)}, u32[]{:S(2)}) collective-permute-start(bf16[128,1024]{1,0:T(8,128)(2,1)S(1)} %fusion.37), channel_id=1, source_target_pairs={{0,16},{4,20},{8,24},{12,28},{16,0},{20,4},{24,8},{28,12},{1,17},{... | collective-permute-start | bytes 786440 | tf_op jit(solution)/shard_map/ppermute | solution.py:290
  260.3 18.1 %collective-permute-start.58 = (bf16[128,1024]{1,0:T(8,128)(2,1)S(1)}, bf16[128,1024]{1,0:T(8,128)(2,1)S(1)}, u32[]{:S(2)}, u32[]{:S(2)}) collective-permute-start(bf16[128,1024]{1,0:T(8,128)(2,1)S(1)} %get-tuple-element.103), channel_id=1, source_target_pairs={{0,8},{4,12},{8,16},{12,20},{16,24},{20,28},{24,0},{28,4},{1,9},{5... | collective-permute-start | bytes 786440 | tf_op jit(solution)/shard_map/ppermute | solution.py:290
  261.2 19.3 %collective-permute-start.57 = (bf16[128,1024]{1,0:T(8,128)(2,1)S(1)}, bf16[128,1024]{1,0:T(8,128)(2,1)S(1)}, u32[]{:S(2)}, u32[]{:S(2)}) collective-permute-start(bf16[128,1024]{1,0:T(8,128)(2,1)S(1)} %get-tuple-element.102), channel_id=1, source_target_pairs={{0,24},{4,28},{8,0},{12,4},{16,8},{20,12},{24,16},{28,20},{1,25},{... | collective-permute-start | bytes 786440 | tf_op jit(solution)/shard_map/ppermute | solution.py:290
  (55 other events, 525.8 us)
where the time goes:
time: 284 us; the launch traced here: 281 us
  waiting for transfers between devices  142 us (50%)
  starting transfers between devices  69.7 us (25%)
  matrix products  21.4 us (8%)
  local copies, waits for them, and re-layouts  20.4 us (7%)
  Pallas kernels  17.1 us (6%)
  other arithmetic  9.9 us (3%)
    ppermute x18, waiting for transfers between devices, zshift(): return lax.ppermute(x, 'sp', pairs)  67.7 us
    ppermute x18, waiting for transfers between devices, crossed(): return lax.ppermute(x, ('sp', 'tp'), pairs)  61.7 us
    ppermute x18, starting transfers between devices, zshift(): return lax.ppermute(x, 'sp', pairs)  26.7 us
    ppermute x18, starting transfers between devices, crossed(): return lax.ppermute(x, ('sp', 'tp'), pairs)  25.7 us
    ppermute x12, starting transfers between devices, across(): return lax.ppermute(x, ('sp', 'tp'), pairs)  16 us
    unnamed x72, local copies, waits for them, and re-layouts  12.2 us
    ppermute x12, waiting for transfers between devices, across(): return lax.ppermute(x, ('sp', 'tp'), pairs)  7.86 us
    dot_general x2, matrix products, expert_sums(): result = jnp.dot(hidden, w_down, preferred_element_type=F32).astype(BF)  7 us
  transfers between devices with their start and end apart: 59, of which 28 were waited for; matrix products, arithmetic and copies ran while one was open for 14% of the time, Pallas kernels for 4%

commit v1 on v0

--- a/solution.py
+++ b/solution.py
@@ -390,7 +390,7 @@
         name="within",
     )(
         query_small, query_large, key_a, key_b, value_rows, *tables, decay, rates,
-        gates.reshape(rows, -1), head_gain.reshape(1, -1),
+        *[after(x, chip_update).reshape(-1, 2 * heads * value_size) for x in (gates, head_gain)],
     )
 
     weight_own = gathered(after(out_weight, theirs))
@@ -399,15 +399,6 @@
     residual_rows = [across(pick(residual_pieces, column_block(j, T)), j) for j in range(T)]
     gain_parts = [across(gain_in, j) for j in range(T)]
 
-    experts = S
-    capacity = 4 * rows // experts
-    one_hot = (routes[:, :, None] == jnp.arange(experts, dtype=jnp.int32)).astype(jnp.int32)
-    one_hot = one_hot.reshape(2 * rows, experts)
-    before = jnp.cumsum(one_hot, axis=0) - one_hot
-    slot_index = jnp.sum(before * one_hot, axis=1).reshape(rows, 2)
-    info = jnp.concatenate(
-        [routes.astype(F32), slot_index.astype(F32), route_weight, route_weight], axis=1
-    )
     state_mine, state_theirs = pl.pallas_call(
         functools.partial(state_kernel, half_a, Z - 1),
         out_shape=(jax.ShapeDtypeStruct((heads, height, value_size), BF),) * 2,
@@ -447,10 +438,19 @@
     ]
     product = jnp.stack([p.reshape(Z, piece, width) for p in products], axis=1)
     outgoing = product.astype(BF)
-    info = after(info, outgoing)
+    moved = [zshift(outgoing[k], -k) for k in range(1, Z)]
+    experts = S
+    capacity = 4 * rows // experts
+    routes, route_weight = after((routes, route_weight), moved)
+    one_hot = (routes[:, :, None] == jnp.arange(experts, dtype=jnp.int32)).astype(jnp.int32)
+    one_hot = one_hot.reshape(2 * rows, experts)
+    before = jnp.cumsum(one_hot, axis=0) - one_hot
+    slot_index = jnp.sum(before * one_hot, axis=1).reshape(rows, 2)
+    info = jnp.concatenate(
+        [routes.astype(F32), slot_index.astype(F32), route_weight, route_weight], axis=1
+    )
     info_pair = jnp.stack([info, swap(info)])
     infos = [zshift(info_pair, k) for k in range(Z)]
-    moved = [zshift(outgoing[k], -k) for k in range(1, Z)]
     *normed, = pl.pallas_call(
         functools.partial(norm_kernel, T, Z - 1),
         out_shape=(jax.ShapeDtypeStruct((piece, T * width), BF),)
@@ -501,8 +501,9 @@
     def expert_rows(group, parts, pieces_first):
         block = jnp.concatenate(parts, axis=0)
         block_other = swap(block)
-        near = jnp.stack([infos[k][0] for k in group])
-        far = jnp.stack([infos[k][1] for k in group])
+        known = after([infos[k] for k in group], block)
+        near = jnp.stack([info[0] for info in known])
+        far = jnp.stack([info[1] for info in known])
         choices = choose(near, first, pieces_first), choose(far, c == 1, pieces_first)
         taken = jnp.concatenate(
             [
@@ -531,7 +532,7 @@
     hidden_odd, near_odd, far_odd = expert_rows(odd, after(parts_odd, hidden_even), True)
     gathered_even = gathered(hidden_even)
     sums_even = expert_sums(even, after(gathered_even, hidden_odd), near_even, far_even)
-    gathered_odd = gathered(hidden_odd)
+    gathered_odd = [hidden_odd] + [across(hidden_odd, j) for j in range(1, T)]
     sums_odd = expert_sums(odd, after(gathered_odd, sums_even), near_odd, far_odd)
     routed = sums_even[0]
     for sums, group in ((sums_even, even), (sums_odd, odd)):

time: 284 us -> 268 us (0.944)
  waiting for transfers between devices: 142 us -> 115 us
  starting transfers between devices: 69.7 us -> 86.1 us
    ppermute x18, waiting for transfers between devices: 67.7 us -> 38.8 us  [zshift(): return lax.ppermute(x, 'sp', pairs)]
    ppermute x18, starting transfers between devices: 26.7 us -> 44.5 us  [zshift(): return lax.ppermute(x, 'sp', pairs)]
    ppermute x18 -> x15, waiting for transfers between devices: 61.7 us -> 47.1 us  [crossed(): return lax.ppermute(x, ('sp', 'tp'), pairs)]
    ppermute x12 -> x15, waiting for transfers between devices: 7.86 us -> 22.4 us  [across(): return lax.ppermute(x, ('sp', 'tp'), pairs)]
    ppermute x18 -> x15, starting transfers between devices: 25.7 us -> 19.7 us  [crossed(): return lax.ppermute(x, ('sp', 'tp'), pairs)]
    ppermute x12 -> x15, starting transfers between devices: 16 us -> 20.2 us  [across(): return lax.ppermute(x, ('sp', 'tp'), pairs)]
    unnamed x72 -> x66, local copies, waits for them, and re-layouts: 12.2 us -> 11.5 us
  transfers between devices with their start and end apart: 59 -> 59, of which waited for: 28 -> 29; matrix products, arithmetic and copies ran while one was open for 14% -> 11% of each run, Pallas kernels for 4% -> 5%
where the time goes in v1:
time: 268 us; the launch traced here: 267 us
  waiting for transfers between devices  115 us (43%)
  starting transfers between devices  86.1 us (32%)
  matrix products  21.2 us (8%)
  local copies, waits for them, and re-layouts  18 us (7%)
  Pallas kernels  17.1 us (6%)
  other arithmetic  7.77 us (3%)
    ppermute x15, waiting for transfers between devices, crossed(): return lax.ppermute(x, ('sp', 'tp'), pairs)  47.1 us
    ppermute x18, starting transfers between devices, zshift(): return lax.ppermute(x, 'sp', pairs)  44.5 us
    ppermute x18, waiting for transfers between devices, zshift(): return lax.ppermute(x, 'sp', pairs)  38.8 us
    ppermute x15, waiting for transfers between devices, across(): return lax.ppermute(x, ('sp', 'tp'), pairs)  22.4 us
    ppermute x15, starting transfers between devices, across(): return lax.ppermute(x, ('sp', 'tp'), pairs)  20.2 us
    ppermute x15, starting transfers between devices, crossed(): return lax.ppermute(x, ('sp', 'tp'), pairs)  19.7 us
    unnamed x66, local copies, waits for them, and re-layouts  11.5 us
    ppermute x11, waiting for transfers between devices, swap(): return lax.ppermute(x, 'sp', [(a, a ^ 1) for a in range(S)])  7.04 us
  transfers between devices with their start and end apart: 59, of which 29 were waited for; matrix products, arithmetic and copies ran while one was open for 11% of the time, Pallas kernels for 5%

profile of v1, /device:TPU:0, one launch (start us, length us, event | category | flops | bytes accessed | tf_op | source)
XLA Modules:
  0.0 266.8 jit_solution(2910517968007606483)
XLA Ops:
  1.7 3.7 %update.1 = (bf16[128,512]{1,0:T(8,128)(2,1)}, bf16[128,1024]{1,0:T(8,128)(2,1)}, f32[4,200,128]{2,1,0:T(8,128)}, f32[4,200,128]{2,1,0:T(8,128)}, f32[128,8]{1,0...) custom-call(bf16[128,512]{1,0:T(8,128)(2,1)} %key_a.1, ...), custom_call_target="tpu_custom_call" | custom-call | tf_op jit(solution)/shard_map/update/pallas_call | solution.py:352
  5.4 3.0 %collective-permute-start.11 = (bf16[2,256,1024]{2,1,0:T(8,128)(2,1)}, bf16[2,256,1024]{2,1,0:T(8,128)(2,1)S(1)}, u32[]{:S(2)}, u32[]{:S(2)}) collective-permute-start(bf16[2,256,1024]{2,1,0:T(8,128)(2,1)} %param.27), channel_id=1, source_target_pairs={{0,1},{1,0},{2,3},{3,2},{4,6},{5,7},{6,4},{7,5},{8,9},{9,8},{10,11... | collective-permute-start | bytes 3145736 | tf_op jit(solution)/shard_map/ppermute | solution.py:308
  9.9 22.2 %collective-permute-done.11 = bf16[2,256,1024]{2,1,0:T(8,128)(2,1)S(1)} collective-permute-done((bf16[2,256,1024]{2,1,0:T(8,128)(2,1)}, bf16[2,256,1024]{2,1,0:T(8,128)(2,1)S(1)}, u32[]{:S(2)}, u32[]{:S(2)}) %collective-permute-start.11) | collective-permute-done | bytes 1048608 | tf_op jit(solution)/shard_map/ppermute | solution.py:308
  36.4 3.5 %collective-permute-start.1 = (bf16[4,208,128]{2,1,0:T(8,128)(2,1)}, bf16[4,208,128]{2,1,0:T(8,128)(2,1)S(1)}, u32[]{:S(2)}, u32[]{:S(2)}) collective-permute-start(bf16[4,208,128]{2,1,0:T(8,128)(2,1)} %chip.1), channel_id=1, source_target_pairs={{0,8},{4,12},{8,16},{12,20},{16,24},{20,28},{1,9},{5,13},{9,17},{1... | collective-permute-start | bytes 638984 | tf_op jit(solution)/shard_map/ppermute | solution.py:290
  39.9 5.2 %collective-permute-start.2 = (bf16[4,208,128]{2,1,0:T(8,128)(2,1)}, bf16[4,208,128]{2,1,0:T(8,128)(2,1)}, u32[]{:S(2)}, u32[]{:S(2)}) collective-permute-start(bf16[4,208,128]{2,1,0:T(8,128)(2,1)} %chip.1), channel_id=1, source_target_pairs={{0,16},{4,20},{8,24},{12,28},{1,17},{5,21},{9,25},{13,29},{2,18},{... | collective-permute-start | bytes 638984 | tf_op jit(solution)/shard_map/ppermute | solution.py:290
  50.0 3.7 %within.1 = (bf16[128,512]{1,0:T(8,128)(2,1)}, bf16[128,1024]{1,0:T(8,128)(2,1)}, f32[128,1024]{1,0:T(8,128)}, f32[128,1024]{1,0:T(8,128)}) custom-call(bf16[128,512]{1,0:T(8,128)(2,1)} %query_a.1, bf16[128,1024]{1,0:T(8,128)(2,1)} %query_b.1, bf16[128,512]{1,0:T(8,128)(2,1)} %get-tuple-element.59.key_a, bf16[128,1024]{1,0:T(8,128)(2,1)} %get-tuple-element.60.key_b, ...), custom_call_target="tpu_custom_call" | custom-call | tf_op jit(solution)/shard_map/within/pallas_call | solution.py:380
  54.4 2.3 state.1
  59.0 3.0 %output.1 = (bf16[32,1024]{1,0:T(8,128)(2,1)}, bf16[32,1024]{1,0:T(8,128)(2,1)}, bf16[32,1024]{1,0:T(8,128)(2,1)}, bf16[32,1024]{1,0:T(8,128)(2,1)}) custom-call(bf16[128,512]{1,0:T(8,128)(2,1)} %get-tuple-element.70.query_a, bf16[128,1024]{1,0:T(8,128)(2,1)} %get-tuple-element.71.query_b, f32[128,1024]{1,0:T(8,128)} %get-tuple-element.72.within, ...), custom_call_target="tpu_custom_call" | custom-call | tf_op jit(solution)/shard_map/output/pallas_call | solution.py:410
  62.1 2.4 collective-permute-start.5
  67.2 2.4 collective-permute-done.6
  72.8 5.6 %collective-permute-start.10 = (bf16[32,1024]{1,0:T(8,128)(2,1)S(1)}, bf16[32,1024]{1,0:T(8,128)(2,1)S(1)}, u32[]{:S(2)}, u32[]{:S(2)}) collective-permute-start(bf16[32,1024]{1,0:T(8,128)(2,1)S(1)} %get-tuple-element.131), channel_id=1, source_target_pairs={{0,24},{4,28},{8,0},{12,4},{16,8},{20,12},{24,16},{28,20},{1,25},{... | collective-permute-start | bytes 196616 | tf_op jit(solution)/shard_map/ppermute | solution.py:290
  94.7 4.5 %collective-permute-done.18.refs_1_ = bf16[4,32,1024]{2,1,0:T(8,128)(2,1)S(1)} collective-permute-done((bf16[4,32,1024]{2,1,0:T(8,128)(2,1)S(1)}, bf16[4,32,1024]{2,1,0:T(8,128)(2,1)S(1)}, u32[]{:S(2)}, u32[]{:S(2)}) %collective-permute-start.18) | collective-permute-done | bytes 262176 | tf_op jit(solution)/shard_map/ppermute | solution.py:290
  99.1 3.6 %collective-permute-start.26 = (f32[1024]{0:T(1024)S(1)}, f32[1024]{0:T(1024)S(1)}, u32[]{:S(2)}, u32[]{:S(2)}) collective-permute-start(f32[1024]{0:T(1024)S(1)} %copy-done.13), channel_id=1, source_target_pairs={{0,3},{1,2},{2,1},{3,0},{4,7},{5,6},{6,5},{7,4},{8,11},{9,10},{10,... | collective-permute-start | bytes 12296 | tf_op jit(solution)/shard_map/ppermute | solution.py:299
  102.7 12.3 %collective-permute-done.19.refs_2_ = bf16[4,32,1024]{2,1,0:T(8,128)(2,1)S(1)} collective-permute-done((bf16[4,32,1024]{2,1,0:T(8,128)(2,1)S(1)}, bf16[4,32,1024]{2,1,0:T(8,128)(2,1)S(1)}, u32[]{:S(2)}, u32[]{:S(2)}) %collective-permute-start.19) | collective-permute-done | bytes 262176 | tf_op jit(solution)/shard_map/ppermute | solution.py:290
  121.0 3.2 %collective-permute-done.23.refs_7_ = bf16[32,1024]{1,0:T(8,128)(2,1)S(1)} collective-permute-done((bf16[32,1024]{1,0:T(8,128)(2,1)S(1)}, bf16[32,1024]{1,0:T(8,128)(2,1)S(1)}, u32[]{:S(2)}, u32[]{:S(2)}) %collective-permute-start.23) | collective-permute-done | bytes 65568 | tf_op jit(solution)/shard_map/ppermute | solution.py:299
  124.8 2.4 norm.1
  132.6 2.9 %collective-permute-start.46 = (bf16[32,4096]{1,0:T(8,128)(2,1)}, bf16[32,4096]{1,0:T(8,128)(2,1)S(1)}, u32[]{:S(2)}, u32[]{:S(2)}) collective-permute-start(bf16[32,4096]{1,0:T(8,128)(2,1)} %get-tuple-element.96), channel_id=1, source_target_pairs={{0,24},{4,28},{8,0},{12,4},{16,8},{20,12},{24,16},{28,20},{1,25},{... | collective-permute-start | bytes 786440 | tf_op jit(solution)/shard_map/ppermute | solution.py:290
  135.5 2.9 %collective-permute-done.45 = bf16[32,4096]{1,0:T(8,128)(2,1)S(1)} collective-permute-done((bf16[32,4096]{1,0:T(8,128)(2,1)}, bf16[32,4096]{1,0:T(8,128)(2,1)S(1)}, u32[]{:S(2)}, u32[]{:S(2)}) %collective-permute-start.45) | collective-permute-done | bytes 262176 | tf_op jit(solution)/shard_map/ppermute | solution.py:290
  138.4 11.3 %collective-permute-start.31 = (f32[2,128,8]{1,2,0:T(8,128)S(1)}, f32[2,128,8]{1,2,0:T(8,128)S(1)}, u32[]{:S(2)}, u32[]{:S(2)}) collective-permute-start(f32[2,128,8]{1,2,0:T(8,128)S(1)} %pad_maximum_fusion.26), channel_id=1, source_target_pairs={{0,16},{4,20},{8,24},{12,28},{16,0},{20,4},{24,8},{28,12},{1,17},{... | collective-permute-start | bytes 24584 | tf_op jit(solution)/shard_map/ppermute | solution.py:290
  149.7 4.0 %collective-permute-start.44 = (f32[2,128,8]{1,2,0:T(8,128)S(1)}, f32[2,128,8]{1,2,0:T(8,128)S(1)}, u32[]{:S(2)}, u32[]{:S(2)}) collective-permute-start(f32[2,128,8]{1,2,0:T(8,128)S(1)} %pad_maximum_fusion.26), channel_id=1, source_target_pairs={{0,24},{4,28},{8,0},{12,4},{16,8},{20,12},{24,16},{28,20},{1,25},{... | collective-permute-start | bytes 24584 | tf_op jit(solution)/shard_map/ppermute | solution.py:290
  156.0 4.3 %collective-permute-done.34 = bf16[32,4096]{1,0:T(8,128)(2,1)S(1)} collective-permute-done((bf16[32,4096]{1,0:T(8,128)(2,1)S(1)}, bf16[32,4096]{1,0:T(8,128)(2,1)S(1)}, u32[]{:S(2)}, u32[]{:S(2)}) %collective-permute-start.34) | collective-permute-done | bytes 262176 | tf_op jit(solution)/shard_map/ppermute | solution.py:308
  161.3 9.4 %collective-permute-done.36 = bf16[32,4096]{1,0:T(8,128)(2,1)S(1)} collective-permute-done((bf16[32,4096]{1,0:T(8,128)(2,1)S(1)}, bf16[32,4096]{1,0:T(8,128)(2,1)S(1)}, u32[]{:S(2)}, u32[]{:S(2)}) %collective-permute-start.36) | collective-permute-done | bytes 262176 | tf_op jit(solution)/shard_map/ppermute | solution.py:308
  171.3 5.8 %collective-permute-done.37 = bf16[32,4096]{1,0:T(8,128)(2,1)S(1)} collective-permute-done((bf16[32,4096]{1,0:T(8,128)(2,1)S(1)}, bf16[32,4096]{1,0:T(8,128)(2,1)S(1)}, u32[]{:S(2)}, u32[]{:S(2)}) %collective-permute-start.37) | collective-permute-done | bytes 262176 | tf_op jit(solution)/shard_map/ppermute | solution.py:308
  179.2 4.2 %collective-permute-done.38 = bf16[32,4096]{1,0:T(8,128)(2,1)S(1)} collective-permute-done((bf16[32,4096]{1,0:T(8,128)(2,1)S(1)}, bf16[32,4096]{1,0:T(8,128)(2,1)S(1)}, u32[]{:S(2)}, u32[]{:S(2)}) %collective-permute-start.38) | collective-permute-done | bytes 262176 | tf_op jit(solution)/shard_map/ppermute | solution.py:308
  186.3 2.4 collective-permute-done.39
  212.6 3.5 %fusion.14 = bf16[256,1024]{1,0:T(8,128)(2,1)S(1)} fusion(bf16[256,2048]{0,1:T(8,128)(2,1)S(1)} %bitcast.252, bf16[1,2048,1024]{2,1,0:T(8,128)(2,1)} %param.33), kind=kOutput, calls=%fused_computation.29 | convolution fusion | flops 1074003968 | bytes 5767168 | tf_op jit(solution)/shard_map/dot_general | solution.py:523
  228.2 5.3 %collective-permute-done.53 = bf16[256,512]{1,0:T(8,128)(2,1)S(1)} collective-permute-done((bf16[256,512]{1,0:T(8,128)(2,1)S(1)}, bf16[256,512]{1,0:T(8,128)(2,1)S(1)}, u32[]{:S(2)}, u32[]{:S(2)}) %collective-permute-start.53) | collective-permute-done | bytes 262176 | tf_op jit(solution)/shard_map/ppermute | solution.py:299
  233.5 5.1 %collective-permute-done.55 = bf16[256,512]{1,0:T(8,128)(2,1)S(1)} collective-permute-done((bf16[256,512]{1,0:T(8,128)(2,1)S(1)}, bf16[256,512]{1,0:T(8,128)(2,1)S(1)}, u32[]{:S(2)}, u32[]{:S(2)}) %collective-permute-start.55) | collective-permute-done | bytes 262176 | tf_op jit(solution)/shard_map/ppermute | solution.py:299
  239.8 3.5 %fusion.17 = bf16[256,1024]{1,0:T(8,128)(2,1)S(1)} fusion(bf16[256,2048]{0,1:T(8,128)(2,1)S(1)} %bitcast.253, bf16[1,2048,1024]{2,1,0:T(8,128)(2,1)} %param.33), kind=kOutput, calls=%fused_computation.30 | convolution fusion | flops 1074003968 | bytes 5767168 | tf_op jit(solution)/shard_map/dot_general | solution.py:523
  246.3 3.8 %collective-permute-start.57 = (bf16[128,1024]{1,0:T(8,128)(2,1)S(1)}, bf16[128,1024]{1,0:T(8,128)(2,1)S(1)}, u32[]{:S(2)}, u32[]{:S(2)}) collective-permute-start(bf16[128,1024]{1,0:T(8,128)(2,1)S(1)} %get-tuple-element.116), channel_id=1, source_target_pairs={{0,24},{4,28},{8,0},{12,4},{16,8},{20,12},{24,16},{28,20},{1,25},{... | collective-permute-start | bytes 786440 | tf_op jit(solution)/shard_map/ppermute | solution.py:290
  250.2 12.5 %collective-permute-done.52 = bf16[128,1024]{1,0:T(8,128)(2,1)S(1)} collective-permute-done((bf16[128,1024]{1,0:T(8,128)(2,1)S(1)}, bf16[128,1024]{1,0:T(8,128)(2,1)S(1)}, u32[]{:S(2)}, u32[]{:S(2)}) %collective-permute-start.52) | collective-permute-done | bytes 262176 | tf_op jit(solution)/shard_map/ppermute | solution.py:290
  262.7 3.1 %collective-permute-done.57 = bf16[128,1024]{1,0:T(8,128)(2,1)S(1)} collective-permute-done((bf16[128,1024]{1,0:T(8,128)(2,1)S(1)}, bf16[128,1024]{1,0:T(8,128)(2,1)S(1)}, u32[]{:S(2)}, u32[]{:S(2)}) %collective-permute-start.57) | collective-permute-done | bytes 262176 | tf_op jit(solution)/shard_map/ppermute | solution.py:290
  (284 shorter events, 98.5 us)
Async XLA Ops:
  5.4 26.7 %collective-permute-start.11 = (bf16[2,256,1024]{2,1,0:T(8,128)(2,1)}, bf16[2,256,1024]{2,1,0:T(8,128)(2,1)S(1)}, u32[]{:S(2)}, u32[]{:S(2)}) collective-permute-start(bf16[2,256,1024]{2,1,0:T(8,128)(2,1)} %param.27), channel_id=1, source_target_pairs={{0,1},{1,0},{2,3},{3,2},{4,6},{5,7},{6,4},{7,5},{8,9},{9,8},{10,11... | collective-permute-start | bytes 3145736 | tf_op jit(solution)/shard_map/ppermute | solution.py:308
  8.4 25.3 %collective-permute-start = (f32[4,200,128]{2,1,0:T(8,128)}, f32[4,200,128]{2,1,0:T(8,128)S(1)}, u32[]{:S(2)}, u32[]{:S(2)}) collective-permute-start(f32[4,200,128]{2,1,0:T(8,128)} %get-tuple-element.67), channel_id=1, source_target_pairs={{0,4},{4,0},{8,12},{12,8},{16,20},{20,16},{24,28},{28,24},{1,5},{5... | collective-permute-start | bytes 1228808 | tf_op jit(solution)/shard_map/ppermute | solution.py:283
  8.4 62.8 %collective-permute-start.12 = (bf16[2,256,1024]{2,1,0:T(8,128)(2,1)}, bf16[2,256,1024]{2,1,0:T(8,128)(2,1)S(1)}, u32[]{:S(2)}, u32[]{:S(2)}) collective-permute-start(bf16[2,256,1024]{2,1,0:T(8,128)(2,1)} %param.27), channel_id=1, source_target_pairs={{0,2},{1,3},{2,0},{3,1},{4,5},{5,4},{6,7},{7,6},{8,10},{9,11},{10,... | collective-permute-start | bytes 3145736 | tf_op jit(solution)/shard_map/ppermute | solution.py:308
  32.1 39.1 %collective-permute-start.13 = (bf16[2,256,1024]{2,1,0:T(8,128)(2,1)S(1)}, bf16[2,256,1024]{2,1,0:T(8,128)(2,1)S(1)}, u32[]{:S(2)}, u32[]{:S(2)}) collective-permute-start(bf16[2,256,1024]{2,1,0:T(8,128)(2,1)S(1)} %collective-permute-done.11), channel_id=1, source_target_pairs={{0,2},{1,3},{2,0},{3,1},{4,5},{5,4},{6,7},{7,6},{8,10},{9,11},{10,... | collective-permute-start | bytes 3145736 | tf_op jit(solution)/shard_map/ppermute | solution.py:308
  36.4 17.3 %collective-permute-start.1 = (bf16[4,208,128]{2,1,0:T(8,128)(2,1)}, bf16[4,208,128]{2,1,0:T(8,128)(2,1)S(1)}, u32[]{:S(2)}, u32[]{:S(2)}) collective-permute-start(bf16[4,208,128]{2,1,0:T(8,128)(2,1)} %chip.1), channel_id=1, source_target_pairs={{0,8},{4,12},{8,16},{12,20},{16,24},{20,28},{1,9},{5,13},{9,17},{1... | collective-permute-start | bytes 638984 | tf_op jit(solution)/shard_map/ppermute | solution.py:290
  39.9 13.8 %collective-permute-start.2 = (bf16[4,208,128]{2,1,0:T(8,128)(2,1)}, bf16[4,208,128]{2,1,0:T(8,128)(2,1)}, u32[]{:S(2)}, u32[]{:S(2)}) collective-permute-start(bf16[4,208,128]{2,1,0:T(8,128)(2,1)} %chip.1), channel_id=1, source_target_pairs={{0,16},{4,20},{8,24},{12,28},{1,17},{5,21},{9,25},{13,29},{2,18},{... | collective-permute-start | bytes 638984 | tf_op jit(solution)/shard_map/ppermute | solution.py:290
  71.2 14.5 %collective-permute-start.17 = (bf16[2,256,1024]{2,1,0:T(8,128)(2,1)S(1)}, bf16[2,256,1024]{2,1,0:T(8,128)(2,1)S(1)}, u32[]{:S(2)}, u32[]{:S(2)}) collective-permute-start(bf16[2,256,1024]{2,1,0:T(8,128)(2,1)S(1)} %collective-permute-done.13), channel_id=1, source_target_pairs={{0,4},{4,0},{8,12},{12,8},{16,20},{20,16},{24,28},{28,24},{1,5},{5... | collective-permute-start | bytes 3145736 | tf_op jit(solution)/shard_map/ppermute | solution.py:283
  72.2 14.5 %collective-permute-start.16 = (bf16[2,256,1024]{2,1,0:T(8,128)(2,1)S(1)}, bf16[2,256,1024]{2,1,0:T(8,128)(2,1)S(1)}, u32[]{:S(2)}, u32[]{:S(2)}) collective-permute-start(bf16[2,256,1024]{2,1,0:T(8,128)(2,1)S(1)} %collective-permute-done.11), channel_id=1, source_target_pairs={{0,4},{4,0},{8,12},{12,8},{16,20},{20,16},{24,28},{28,24},{1,5},{5... | collective-permute-start | bytes 3145736 | tf_op jit(solution)/shard_map/ppermute | solution.py:283
  80.9 38.1 %collective-permute-start.24 = (f32[1024]{0:T(1024)S(1)}, f32[1024]{0:T(1024)S(1)}, u32[]{:S(2)}, u32[]{:S(2)}) collective-permute-start(f32[1024]{0:T(1024)S(1)} %copy-done.13), channel_id=1, source_target_pairs={{0,1},{1,0},{2,3},{3,2},{4,6},{5,7},{6,4},{7,5},{8,9},{9,8},{10,11... | collective-permute-start | bytes 12296 | tf_op jit(solution)/shard_map/ppermute | solution.py:299
  84.9 35.3 %collective-permute-start.25 = (f32[1024]{0:T(1024)S(1)}, f32[1024]{0:T(1024)S(1)}, u32[]{:S(2)}, u32[]{:S(2)}) collective-permute-start(f32[1024]{0:T(1024)S(1)} %copy-done.13), channel_id=1, source_target_pairs={{0,2},{1,3},{2,0},{3,1},{4,5},{5,4},{6,7},{7,6},{8,10},{9,11},{10,... | collective-permute-start | bytes 12296 | tf_op jit(solution)/shard_map/ppermute | solution.py:299
  92.2 22.8 %collective-permute-start.19 = (bf16[4,32,1024]{2,1,0:T(8,128)(2,1)S(1)}, bf16[4,32,1024]{2,1,0:T(8,128)(2,1)S(1)}, u32[]{:S(2)}, u32[]{:S(2)}) collective-permute-start(bf16[4,32,1024]{2,1,0:T(8,128)(2,1)S(1)} %get-tuple-element.114), channel_id=1, source_target_pairs={{0,16},{4,20},{8,24},{12,28},{16,0},{20,4},{24,8},{28,12},{1,17},{... | collective-permute-start | bytes 786440 | tf_op jit(solution)/shard_map/ppermute | solution.py:290
  92.2 24.5 %collective-permute-start.20 = (bf16[4,32,1024]{2,1,0:T(8,128)(2,1)S(1)}, bf16[4,32,1024]{2,1,0:T(8,128)(2,1)S(1)}, u32[]{:S(2)}, u32[]{:S(2)}) collective-permute-start(bf16[4,32,1024]{2,1,0:T(8,128)(2,1)S(1)} %get-tuple-element.113), channel_id=1, source_target_pairs={{0,8},{4,12},{8,16},{12,20},{16,24},{20,28},{24,0},{28,4},{1,9},{5... | collective-permute-start | bytes 786440 | tf_op jit(solution)/shard_map/ppermute | solution.py:290
  99.1 21.1 %collective-permute-start.26 = (f32[1024]{0:T(1024)S(1)}, f32[1024]{0:T(1024)S(1)}, u32[]{:S(2)}, u32[]{:S(2)}) collective-permute-start(f32[1024]{0:T(1024)S(1)} %copy-done.13), channel_id=1, source_target_pairs={{0,3},{1,2},{2,1},{3,0},{4,7},{5,6},{6,5},{7,4},{8,11},{9,10},{10,... | collective-permute-start | bytes 12296 | tf_op jit(solution)/shard_map/ppermute | solution.py:299
  120.2 12.4 %collective-permute-start.30 = (f32[128,8]{0,1:T(8,128)S(1)}, f32[128,8]{0,1:T(8,128)S(1)}, u32[]{:S(2)}, u32[]{:S(2)}) collective-permute-start(f32[128,8]{0,1:T(8,128)S(1)} %get-tuple-element.151), channel_id=1, source_target_pairs={{0,4},{4,0},{8,12},{12,8},{16,20},{20,16},{24,28},{28,24},{1,5},{5... | collective-permute-start | bytes 12296 | tf_op jit(solution)/shard_map/ppermute | solution.py:283
  127.2 11.2 %collective-permute-start.45 = (bf16[32,4096]{1,0:T(8,128)(2,1)}, bf16[32,4096]{1,0:T(8,128)(2,1)S(1)}, u32[]{:S(2)}, u32[]{:S(2)}) collective-permute-start(bf16[32,4096]{1,0:T(8,128)(2,1)} %get-tuple-element.96), channel_id=1, source_target_pairs={{0,8},{4,12},{8,16},{12,20},{16,24},{20,28},{24,0},{28,4},{1,9},{5... | collective-permute-start | bytes 786440 | tf_op jit(solution)/shard_map/ppermute | solution.py:290
  128.2 21.5 %collective-permute-start.32 = (bf16[32,4096]{1,0:T(8,128)(2,1)}, bf16[32,4096]{1,0:T(8,128)(2,1)S(1)}, u32[]{:S(2)}, u32[]{:S(2)}) collective-permute-start(bf16[32,4096]{1,0:T(8,128)(2,1)} %get-tuple-element.96), channel_id=1, source_target_pairs={{0,1},{1,0},{2,3},{3,2},{4,6},{5,7},{6,4},{7,5},{8,9},{9,8},{10,11... | collective-permute-start | bytes 786440 | tf_op jit(solution)/shard_map/ppermute | solution.py:308
  129.6 20.1 %collective-permute-start.33 = (bf16[32,4096]{1,0:T(8,128)(2,1)}, bf16[32,4096]{1,0:T(8,128)(2,1)S(1)}, u32[]{:S(2)}, u32[]{:S(2)}) collective-permute-start(bf16[32,4096]{1,0:T(8,128)(2,1)} %get-tuple-element.96), channel_id=1, source_target_pairs={{0,2},{1,3},{2,0},{3,1},{4,5},{5,4},{6,7},{7,6},{8,10},{9,11},{10,... | collective-permute-start | bytes 786440 | tf_op jit(solution)/shard_map/ppermute | solution.py:308
  130.6 24.2 %collective-permute-start.35 = (bf16[32,4096]{1,0:T(8,128)(2,1)}, bf16[32,4096]{1,0:T(8,128)(2,1)S(1)}, u32[]{:S(2)}, u32[]{:S(2)}) collective-permute-start(bf16[32,4096]{1,0:T(8,128)(2,1)} %get-tuple-element.96), channel_id=1, source_target_pairs={{0,16},{4,20},{8,24},{12,28},{16,0},{20,4},{24,8},{28,12},{1,17},{... | collective-permute-start | bytes 786440 | tf_op jit(solution)/shard_map/ppermute | solution.py:290
  132.6 21.2 %collective-permute-start.46 = (bf16[32,4096]{1,0:T(8,128)(2,1)}, bf16[32,4096]{1,0:T(8,128)(2,1)S(1)}, u32[]{:S(2)}, u32[]{:S(2)}) collective-permute-start(bf16[32,4096]{1,0:T(8,128)(2,1)} %get-tuple-element.96), channel_id=1, source_target_pairs={{0,24},{4,28},{8,0},{12,4},{16,8},{20,12},{24,16},{28,20},{1,25},{... | collective-permute-start | bytes 786440 | tf_op jit(solution)/shard_map/ppermute | solution.py:290
  138.4 45.7 %collective-permute-start.31 = (f32[2,128,8]{1,2,0:T(8,128)S(1)}, f32[2,128,8]{1,2,0:T(8,128)S(1)}, u32[]{:S(2)}, u32[]{:S(2)}) collective-permute-start(f32[2,128,8]{1,2,0:T(8,128)S(1)} %pad_maximum_fusion.26), channel_id=1, source_target_pairs={{0,16},{4,20},{8,24},{12,28},{16,0},{20,4},{24,8},{28,12},{1,17},{... | collective-permute-start | bytes 24584 | tf_op jit(solution)/shard_map/ppermute | solution.py:290
  149.6 50.3 %collective-permute-start.43 = (f32[2,128,8]{1,2,0:T(8,128)S(1)}, f32[2,128,8]{1,2,0:T(8,128)S(1)}, u32[]{:S(2)}, u32[]{:S(2)}) collective-permute-start(f32[2,128,8]{1,2,0:T(8,128)S(1)} %pad_maximum_fusion.26), channel_id=1, source_target_pairs={{0,8},{4,12},{8,16},{12,20},{16,24},{20,28},{24,0},{28,4},{1,9},{5... | collective-permute-start | bytes 24584 | tf_op jit(solution)/shard_map/ppermute | solution.py:290
  149.7 50.2 %collective-permute-start.44 = (f32[2,128,8]{1,2,0:T(8,128)S(1)}, f32[2,128,8]{1,2,0:T(8,128)S(1)}, u32[]{:S(2)}, u32[]{:S(2)}) collective-permute-start(f32[2,128,8]{1,2,0:T(8,128)S(1)} %pad_maximum_fusion.26), channel_id=1, source_target_pairs={{0,24},{4,28},{8,0},{12,4},{16,8},{20,12},{24,16},{28,20},{1,25},{... | collective-permute-start | bytes 24584 | tf_op jit(solution)/shard_map/ppermute | solution.py:290
  154.9 22.8 %collective-permute-start.47 = (bf16[64,4096]{1,0:T(8,128)(2,1)S(1)}, bf16[64,4096]{1,0:T(8,128)(2,1)S(1)}, u32[]{:S(2)}, u32[]{:S(2)}) collective-permute-start(bf16[64,4096]{1,0:T(8,128)(2,1)S(1)} %constant_dynamic-update-slice_fusion.8), channel_id=1, source_target_pairs={{0,1},{1,0},{2,3},{3,2},{4,6},{5,7},{6,4},{7,5},{8,9},{9,8},{10,11... | collective-permute-start | bytes 1572872 | tf_op jit(solution)/shard_map/ppermute | solution.py:308
  160.4 10.4 %collective-permute-start.36 = (bf16[32,4096]{1,0:T(8,128)(2,1)S(1)}, bf16[32,4096]{1,0:T(8,128)(2,1)S(1)}, u32[]{:S(2)}, u32[]{:S(2)}) collective-permute-start(bf16[32,4096]{1,0:T(8,128)(2,1)S(1)} %collective-permute-done.35), channel_id=1, source_target_pairs={{0,1},{1,0},{2,3},{3,2},{4,6},{5,7},{6,4},{7,5},{8,9},{9,8},{10,11... | collective-permute-start | bytes 786440 | tf_op jit(solution)/shard_map/ppermute | solution.py:308
  177.7 18.3 %collective-permute-start.48 = (bf16[64,4096]{1,0:T(8,128)(2,1)S(1)}, bf16[64,4096]{1,0:T(8,128)(2,1)}, u32[]{:S(2)}, u32[]{:S(2)}) collective-permute-start(bf16[64,4096]{1,0:T(8,128)(2,1)S(1)} %constant_dynamic-update-slice_fusion.8), channel_id=1, source_target_pairs={{0,2},{1,3},{2,0},{3,1},{4,5},{5,4},{6,7},{7,6},{8,10},{9,11},{10,... | collective-permute-start | bytes 1572872 | tf_op jit(solution)/shard_map/ppermute | solution.py:308
  183.5 14.2 %collective-permute-start.49 = (bf16[64,4096]{1,0:T(8,128)(2,1)S(1)}, bf16[64,4096]{1,0:T(8,128)(2,1)}, u32[]{:S(2)}, u32[]{:S(2)}) collective-permute-start(bf16[64,4096]{1,0:T(8,128)(2,1)S(1)} %collective-permute-done.47), channel_id=1, source_target_pairs={{0,2},{1,3},{2,0},{3,1},{4,5},{5,4},{6,7},{7,6},{8,10},{9,11},{10,... | collective-permute-start | bytes 1572872 | tf_op jit(solution)/shard_map/ppermute | solution.py:308
  196.0 14.1 %collective-permute-start.41 = (bf16[256,512]{1,0:T(8,128)(2,1)S(1)}, bf16[256,512]{1,0:T(8,128)(2,1)}, u32[]{:S(2)}, u32[]{:S(2)}) collective-permute-start(bf16[256,512]{1,0:T(8,128)(2,1)S(1)} %fusion.29), channel_id=1, source_target_pairs={{0,2},{1,3},{2,0},{3,1},{4,5},{5,4},{6,7},{7,6},{8,10},{9,11},{10,... | collective-permute-start | bytes 786440 | tf_op jit(solution)/shard_map/ppermute | solution.py:308
  216.6 11.2 %collective-permute-start.51 = (bf16[2,128,1024]{2,1,0:T(8,128)(2,1)S(1)}, bf16[2,128,1024]{2,1,0:T(8,128)(2,1)S(1)}, u32[]{:S(2)}, u32[]{:S(2)}) collective-permute-start(bf16[2,128,1024]{2,1,0:T(8,128)(2,1)S(1)} %fusion.12), channel_id=1, source_target_pairs={{0,4},{4,0},{8,12},{12,8},{16,20},{20,16},{24,28},{28,24},{1,5},{5... | collective-permute-start | bytes 1572872 | tf_op jit(solution)/shard_map/ppermute | solution.py:283
  226.3 12.4 %collective-permute-start.55 = (bf16[256,512]{1,0:T(8,128)(2,1)S(1)}, bf16[256,512]{1,0:T(8,128)(2,1)S(1)}, u32[]{:S(2)}, u32[]{:S(2)}) collective-permute-start(bf16[256,512]{1,0:T(8,128)(2,1)S(1)} %fusion.26), channel_id=1, source_target_pairs={{0,3},{1,2},{2,1},{3,0},{4,7},{5,6},{6,5},{7,4},{8,11},{9,10},{10,... | collective-permute-start | bytes 786440 | tf_op jit(solution)/shard_map/ppermute | solution.py:299
  243.9 18.8 %collective-permute-start.52 = (bf16[128,1024]{1,0:T(8,128)(2,1)S(1)}, bf16[128,1024]{1,0:T(8,128)(2,1)S(1)}, u32[]{:S(2)}, u32[]{:S(2)}) collective-permute-start(bf16[128,1024]{1,0:T(8,128)(2,1)S(1)} %fusion.37), channel_id=1, source_target_pairs={{0,16},{4,20},{8,24},{12,28},{16,0},{20,4},{24,8},{28,12},{1,17},{... | collective-permute-start | bytes 786440 | tf_op jit(solution)/shard_map/ppermute | solution.py:290
  246.2 16.5 %collective-permute-start.58 = (bf16[128,1024]{1,0:T(8,128)(2,1)S(1)}, bf16[128,1024]{1,0:T(8,128)(2,1)S(1)}, u32[]{:S(2)}, u32[]{:S(2)}) collective-permute-start(bf16[128,1024]{1,0:T(8,128)(2,1)S(1)} %get-tuple-element.117), channel_id=1, source_target_pairs={{0,8},{4,12},{8,16},{12,20},{16,24},{20,28},{24,0},{28,4},{1,9},{5... | collective-permute-start | bytes 786440 | tf_op jit(solution)/shard_map/ppermute | solution.py:290
  246.3 19.5 %collective-permute-start.57 = (bf16[128,1024]{1,0:T(8,128)(2,1)S(1)}, bf16[128,1024]{1,0:T(8,128)(2,1)S(1)}, u32[]{:S(2)}, u32[]{:S(2)}) collective-permute-start(bf16[128,1024]{1,0:T(8,128)(2,1)S(1)} %get-tuple-element.116), channel_id=1, source_target_pairs={{0,24},{4,28},{8,0},{12,4},{16,8},{20,12},{24,16},{28,20},{1,25},{... | collective-permute-start | bytes 786440 | tf_op jit(solution)/shard_map/ppermute | solution.py:290
  (53 other events, 404.4 us)
